TPU v7x, 32 devices: a whole 2x2x4 slice. The times are simulated.
32 devices in a mesh: sp: 8 (over z, y), tp: 4 (over x, core).
Axes of the slice: x: 2, y: 2, z: 4, core: 2. Of those that a mesh axis runs over, the one named last changes fastest.
Arguments:
- hidden_in: bfloat16 [6144, 4096], P('sp', 'tp'), may hold values from -16 to 16
- norm_gain: bfloat16 [2, 4096], P(None, 'tp'), may hold values from 0.099609375 to 1.8984375
- value_proj: bfloat16 [2, 4096, 1024], P(None, 'tp', 'sp'), may hold values from -0.09375 to 0.09375
- gate_proj: bfloat16 [2, 4096, 1024], P(None, 'tp', 'sp'), may hold values from -0.09375 to 0.09375
- conv_taps: bfloat16 [2, 31, 1024], P(None, None, 'tp'), may hold values from -1 to 1
- conv_bias: bfloat16 [2, 1024], P(None, 'tp'), may hold values from -3 to 3
- group_gain: bfloat16 [2, 1024], P(None, 'tp'), may hold values from 0.099609375 to 1.8984375
- group_shift: bfloat16 [2, 1024], P(None, 'tp'), may hold values from -3 to 3
- out_proj: bfloat16 [2, 1024, 4096], P(None, 'sp', 'tp'), may hold values from -0.1875 to 0.1875
Outputs:
- hidden_out: bfloat16 [6144, 4096], P('sp', 'tp')
All inputs are finite; a program needn't handle non-finite values.
Results may differ from a plain program's by a relative error of at most 0.012.
Values may be sent and summed in bfloat16 or wider, within the bound.
A program may use at most 128 MiB of HBM per device.

v0:
```python
import jax
import jax.numpy as jnp
from jax import lax
from jax.experimental import pallas as pl
from jax.experimental.pallas import tpu as pltpu
from jax.sharding import PartitionSpec as P

D = 4096
C = 1024
GROUPS = 4
WIDTH = 31


row_floor = 1e-06
group_floor = 1e-05


def passed_along(value, axis, steps):
    count = lax.axis_size(axis)
    initial, last = (max(0, -steps), min(count, count - steps))
    return lax.ppermute(value, axis, [(source, source + steps) for source in range(initial, last)])


def rms_normed(residual_rows, gain_part):
    wide_rows = residual_rows.astype(jnp.float32)
    squares = lax.psum(jnp.sum(wide_rows * wide_rows, axis=1), "tp")
    scale_rows = lax.rsqrt(squares / D + row_floor)
    return (wide_rows * scale_rows[:, None] * gain_part.astype(jnp.float32)[None, :]).astype(
        jnp.bfloat16
    )


def gated_input(normed_rows, w_value, w_gate):
    numbers = (((0,), (1,)), ((), ()))
    value_part = lax.dot_general(w_value, normed_rows, numbers, preferred_element_type=jnp.float32)
    gate_part = lax.dot_general(w_gate, normed_rows, numbers, preferred_element_type=jnp.float32)
    summed = lax.psum_scatter(
        jnp.stack([value_part, gate_part], axis=1).astype(jnp.bfloat16),
        "tp",
        scatter_dimension=0,
        tiled=True,
    ).astype(jnp.float32)
    return (summed[:, 0] * jax.nn.sigmoid(summed[:, 1])).astype(jnp.bfloat16)


def depthwise(extended, taps_part, bias_part, out_len):
    widened = extended.astype(jnp.float32)
    taps = taps_part.astype(jnp.float32)
    filtered = (
        jnp.zeros((extended.shape[0], out_len), jnp.float32)
        + bias_part.astype(jnp.float32)[:, None]
    )
    for offset in range(WIDTH):
        filtered = filtered + taps[offset][:, None] * widened[:, offset : offset + out_len]
    return filtered


def group_normed(filtered, gain_part, shift_part, group_size):
    channels, out_len = filtered.shape
    grouped = filtered.reshape(channels // group_size, group_size, out_len)
    group_mean = jnp.mean(grouped, axis=1, keepdims=True)
    centered = grouped - group_mean
    group_var = jnp.mean(centered * centered, axis=1, keepdims=True)
    scaled = (centered * lax.rsqrt(group_var + group_floor)).reshape(channels, out_len)
    scaled = (
        scaled * gain_part.astype(jnp.float32)[:, None] + shift_part.astype(jnp.float32)[:, None]
    )
    return jax.nn.silu(scaled).astype(jnp.bfloat16)


def project_out(mixed, w_out):
    return lax.dot_general(
        lax.all_gather(mixed, "tp", axis=0, tiled=True),
        w_out,
        (((0,), (0,)), ((), ())),
        preferred_element_type=jnp.float32,
    )


def on_device(
    hidden_in,
    norm_gain,
    value_proj,
    gate_proj,
    conv_taps,
    conv_bias,
    group_gain,
    group_shift,
    out_proj,
):
    tok_rows = hidden_in.shape[0]
    layers = norm_gain.shape[0]
    reach_back = WIDTH - 1
    group_size = C // GROUPS
    all_value, all_gate, all_out = (
        lax.all_gather(value_proj, "sp", axis=2, tiled=True),
        lax.all_gather(gate_proj, "sp", axis=2, tiled=True),
        lax.all_gather(out_proj, "sp", axis=1, tiled=True),
    )
    residual_rows = hidden_in
    for level in range(layers):
        w_value, w_gate, w_out = (all_value[level], all_gate[level], all_out[level])
        normed_rows = rms_normed(residual_rows, norm_gain[level])
        gated = gated_input(normed_rows, w_value, w_gate)
        before = passed_along(gated[:, tok_rows - reach_back :], "sp", 1)
        extended = jnp.concatenate([before, gated], axis=1)
        out_len = extended.shape[1] - reach_back
        filtered = depthwise(extended, conv_taps[level], conv_bias[level], out_len)
        mixed = group_normed(filtered, group_gain[level], group_shift[level], group_size)
        update = project_out(mixed, w_out)
        kept_rows = residual_rows
        residual_rows = (kept_rows.astype(jnp.float32) + update).astype(jnp.bfloat16)
    return residual_rows


MESH = pl.DeviceIdType.MESH
HALO = 32
ROW_TILE = 256
CONV_TILE = 64
VMEM_BYTES = 62 * 1024 * 1024
SPLIT = 3


def fused_kernel(
    n_sp,
    n_tp,
    hidden_ref,
    norm_ref,
    value_ref,
    gate_ref,
    taps_ref,
    bias_ref,
    ggain_ref,
    gshift_ref,
    out_proj_ref,
    out_ref,
    w_in,
    w_out,
    scaled,
    part,
    from_core,
    to_chip,
    from_chip,
    extended,
    halo_send,
    halo_recv,
    mixed,
    squares,
    load_sem,
    w_send,
    w_recv,
    t_send,
    t_recv,
    s_send,
    s_recv,
):
    layers, width = taps_ref.shape[0], taps_ref.shape[1]
    rows, feats = hidden_ref.shape
    piece = value_ref.shape[2]
    blocks = n_sp // n_tp
    channels = blocks * piece
    reach = width - 1
    nz = n_sp // 2
    s = lax.axis_index("sp")
    t = lax.axis_index("tp")
    z, y = s // 2, s % 2
    chip, core = t // 2, t % 2
    core_mate = chip * 2 + (1 - core)
    chip_mate = (1 - chip) * 2 + core
    far_mate = (1 - chip) * 2 + (1 - core)

    loads = []
    for level in range(layers):
        for kind, (source, target) in enumerate(
            (
                (value_ref.at[level], w_in.at[level, s, :, pl.ds(0, piece)]),
                (gate_ref.at[level], w_in.at[level, s, :, pl.ds(piece, piece)]),
                (
                    out_proj_ref.at[level],
                    w_out.at[level, pl.ds(pl.multiple_of(s * piece, piece), piece), :],
                ),
            )
        ):
            copy = pltpu.make_async_copy(source, target, load_sem.at[level, kind])
            copy.start()
            loads.append(copy)

    barrier = pltpu.get_barrier_semaphore()

    def greet(sp_index, tp_index):
        pl.semaphore_signal(barrier, inc=1, device_id=(sp_index, tp_index), device_id_type=MESH)

    up, down = z < nz - 1, z > 0
    corner_up = jnp.logical_and(up, y == 1)
    corner_down = jnp.logical_and(down, y == 0)
    for mate in (core_mate, chip_mate, far_mate):
        greet(s, mate)
    greet(z * 2 + 1 - y, t)
    for condition, target in (
        (up, s + 2),
        (down, s - 2),
        (corner_up, s + 1),
        (corner_down, s - 1),
    ):

        @pl.when(condition)
        def _(target=target):
            greet(target, t)

    mates = 4
    for condition in (up, down, corner_up, corner_down):
        mates = mates + condition.astype(jnp.int32)
    pl.semaphore_wait(barrier, mates)

    for copy in loads:
        copy.wait()

    half = feats // 2
    phases = []
    for level in range(layers):
        phases += [("in", level, 0), ("in", level, 1), ("out", level, 0)]

    def chunk(phase, owner, lot):
        kind, level, part_index = phases[phase]
        deep = half if kind == "in" else piece
        cut = deep - deep * SPLIT // 16 // 16 * 16
        low, size = (0, cut) if lot == 0 else (cut, deep - cut)
        if kind == "in":
            return w_in.at[level, owner, pl.ds(part_index * half + low, size), :]
        return w_out.at[level, pl.ds(pl.multiple_of(owner * piece, piece) + low, size), :]

    def weight_copy(phase, owner, way, lot):
        target = (s + 2, s - 2, z * 2 + 1 - y)[way]
        return pltpu.make_async_remote_copy(
            src_ref=chunk(phase, owner, lot),
            dst_ref=chunk(phase, owner, lot),
            send_sem=w_send.at[phase, lot, way, owner],
            recv_sem=w_recv.at[phase, lot, owner],
            device_id=(target, t),
            device_id_type=MESH,
        )

    def both_ways(phase, owner, lot):
        @pl.when(up)
        def _():
            weight_copy(phase, owner, 0, lot).start()

        @pl.when(down)
        def _():
            weight_copy(phase, owner, 1, lot).start()

    def own(phase):
        for lot in (1, 0):
            weight_copy(phase, s, 2, lot).start()
            both_ways(phase, s, lot)

    def hops(phase):
        across = z * 2 + 1 - y
        weight_copy(phase, across, 2, 1).wait_recv()
        both_ways(phase, across, 1)
        moves = ((y, 1), (y, 0), (1 - y, 1))
        for hop in range(1, nz):
            for column, lot in moves:

                @pl.when(z >= hop)
                def _(hop=hop, column=column, lot=lot):
                    owner = (z - hop) * 2 + column
                    weight_copy(phase, owner, 0, lot).wait_recv()

                    @pl.when(up)
                    def _():
                        weight_copy(phase, owner, 0, lot).start()

                    if lot == 0:
                        weight_copy(phase, owner, 2, lot).start()

                @pl.when(z + hop < nz)
                def _(hop=hop, column=column, lot=lot):
                    owner = (z + hop) * 2 + column
                    weight_copy(phase, owner, 1, lot).wait_recv()

                    @pl.when(down)
                    def _():
                        weight_copy(phase, owner, 1, lot).start()

                    if lot == 0:
                        weight_copy(phase, owner, 2, lot).start()

    def crossed(phase):
        for z_from in range(nz):
            weight_copy(phase, z_from * 2 + 1 - y, 2, 0).wait_recv()

    def sent(phase):
        for z_from in range(nz):
            for column, lot in ((y, 0), (y, 1), (1 - y, 1)):
                owner = z_from * 2 + column

                @pl.when(jnp.logical_and(z >= z_from, up))
                def _(owner=owner, lot=lot):
                    weight_copy(phase, owner, 0, lot).wait_send()

                @pl.when(jnp.logical_and(z <= z_from, down))
                def _(owner=owner, lot=lot):
                    weight_copy(phase, owner, 1, lot).wait_send()

            weight_copy(phase, z_from * 2 + y, 2, 0).wait_send()
        weight_copy(phase, s, 2, 1).wait_send()

    def tp_copy(level, slot, source, target, mate, sp_index=None):
        return pltpu.make_async_remote_copy(
            src_ref=source,
            dst_ref=target,
            send_sem=t_send.at[level, slot],
            recv_sem=t_recv.at[level, slot],
            device_id=(s if sp_index is None else sp_index, mate),
            device_id_type=MESH,
        )

    def prepare(level):
        gain = norm_ref[pl.ds(level, 1), :].astype(jnp.float32)
        ones = jnp.ones((8, feats), jnp.bfloat16)
        numbers = (((1,), (1,)), ((), ()))
        source = hidden_ref if level == 0 else out_ref
        for tile in range(rows // ROW_TILE):
            span = pl.ds(tile * ROW_TILE, ROW_TILE)
            wide = source[span, :].astype(jnp.float32)
            scaled[span, :] = (wide * gain).astype(jnp.bfloat16)
            square = wide * wide
            high = square.astype(jnp.bfloat16)
            low = (square - high.astype(jnp.float32)).astype(jnp.bfloat16)
            total = lax.dot_general(ones, high, numbers, preferred_element_type=jnp.float32)
            total = total + lax.dot_general(ones, low, numbers, preferred_element_type=jnp.float32)
            squares[level, t, :, span] = total
        for slot, mate in enumerate((core_mate, chip_mate, far_mate)):
            square_copy(level, slot, mate).start()

    def square_copy(level, slot, mate):
        return pltpu.make_async_remote_copy(
            src_ref=squares.at[level, t],
            dst_ref=squares.at[level, t],
            send_sem=s_send.at[level, slot],
            recv_sem=s_recv.at[level, slot],
            device_id=(s, mate),
            device_id_type=MESH,
        )

    def row_scales(level):
        for slot, mate in enumerate((core_mate, chip_mate, far_mate)):
            copy = square_copy(level, slot, mate)
            copy.wait_send()
            copy.wait_recv()
        total = squares[level, 0]
        for index in range(1, n_tp):
            total = total + squares[level, index]
        scale = lax.rsqrt(total / D + row_floor)
        return scale.T[:, 0:1]

    def products(level, owner):
        @pl.loop(0, blocks * (rows // ROW_TILE))
        def _(step):
            block = step // (rows // ROW_TILE)
            tile = step % (rows // ROW_TILE)
            span = pl.ds(pl.multiple_of(tile * ROW_TILE, ROW_TILE), ROW_TILE)
            part[owner, block, span, :] = jnp.dot(
                scaled[span, :],
                w_in[level, owner * blocks + block],
                preferred_element_type=jnp.float32,
            ).astype(jnp.bfloat16)

    base = 2 + blocks
    parts = rows // ROW_TILE
    order = tuple(reversed(range(parts)))

    def core_copy(level, slot):
        owner = (far_mate, core_mate)[slot]
        return tp_copy(level, slot, part.at[owner], from_core.at[level, slot], core_mate)

    def chip_copy(level, block):
        return tp_copy(
            level, 2 + block, to_chip.at[block], from_chip.at[level, block], chip_mate
        )

    def halo_copy(level):
        return tp_copy(level, base + 3 * parts, halo_send, halo_recv.at[level], t, s + 1)

    def mixed_copy(level, slot, third):
        owner = (t, t, chip_mate)[slot]
        mate = (core_mate, chip_mate, core_mate)[slot]
        block = mixed.at[level, owner, pl.ds(third * ROW_TILE, ROW_TILE), :]
        return tp_copy(level, base + slot * parts + third, block, block, mate)

    def first_half(level):
        products(level, far_mate)
        core_copy(level, 0).start()
        products(level, chip_mate)
        core_copy(level, 0).wait_recv()
        for block in range(blocks):
            to_chip[block] = (
                part[chip_mate, block].astype(jnp.float32)
                + from_core[level, 0, block].astype(jnp.float32)
            ).astype(jnp.bfloat16)
            chip_copy(level, block).start()
        products(level, core_mate)
        core_copy(level, 1).start()
        products(level, t)
        core_copy(level, 1).wait_recv()

    def gating(level):
        scale = row_scales(level)
        for block in range(blocks):
            lanes = pl.ds(block * piece, piece)
            chip_copy(level, block).wait_recv()
            total = (
                part[t, block].astype(jnp.float32)
                + from_core[level, 1, block].astype(jnp.float32)
                + from_chip[level, block].astype(jnp.float32)
            ) * scale
            gated = (total[:, :piece] * jax.nn.sigmoid(total[:, piece:])).astype(jnp.bfloat16)
            halo_send[:, lanes] = gated[rows - HALO :]
            extended[pl.ds(HALO, rows), lanes] = gated.astype(jnp.float32)

        @pl.when(s < n_sp - 1)
        def _():
            halo_copy(level).start()

    def filtering(level):
        taps = taps_ref[level].astype(jnp.float32)
        bias = bias_ref[pl.ds(level, 1), :].astype(jnp.float32)
        ggain = ggain_ref[pl.ds(level, 1), :].astype(jnp.float32)
        gshift = gshift_ref[pl.ds(level, 1), :].astype(jnp.float32)

        per_part = ROW_TILE // CONV_TILE
        for third in order:
            if third == 0:
                @pl.when(s > 0)
                def _():
                    halo_copy(level).wait_recv()
                    extended[pl.ds(0, HALO), :] = halo_recv[level].astype(jnp.float32)

                @pl.when(s == 0)
                def _():
                    extended[pl.ds(0, HALO), :] = jnp.zeros((HALO, channels), jnp.float32)

            @pl.loop(third * per_part, (third + 1) * per_part)
            def _(tile):
                start = pl.multiple_of(tile * CONV_TILE, CONV_TILE)
                window = extended[pl.ds(start, CONV_TILE + HALO), :]
                filtered = jnp.zeros((CONV_TILE, channels), jnp.float32) + bias
                for offset in range(width):
                    low = HALO - reach + offset
                    filtered = filtered + taps[offset : offset + 1, :] * window[low : low + CONV_TILE]
                mean = jnp.mean(filtered, axis=1, keepdims=True)
                centered = filtered - mean
                var = jnp.mean(centered * centered, axis=1, keepdims=True)
                normed = centered * lax.rsqrt(var + group_floor) * ggain + gshift
                mixed[level, t, pl.ds(start, CONV_TILE), :] = (
                    normed * jax.nn.sigmoid(normed)
                ).astype(jnp.bfloat16)

            mixed_copy(level, 1, third).start()
            mixed_copy(level, 0, third).start()

    def relay(level, third):
        mixed_copy(level, 1, third).wait_recv()
        mixed_copy(level, 2, third).start()

    def projecting(level, third):
        mixed_copy(level, 0, third).wait_recv()
        mixed_copy(level, 2, third).wait_recv()
        source = hidden_ref if level == 0 else out_ref
        span = pl.ds(third * ROW_TILE, ROW_TILE)
        total = source[span, :].astype(jnp.float32)
        for owner in range(n_tp):
            total = total + jnp.dot(
                mixed[level, owner, span, :],
                w_out[level, pl.ds(owner * channels, channels), :],
                preferred_element_type=jnp.float32,
            )
        out_ref[span, :] = total.astype(jnp.bfloat16)

    def settle(level):
        for slot in range(2):
            core_copy(level, slot).wait_send()
        for block in range(blocks):
            chip_copy(level, block).wait_send()
        for slot in range(3):
            for third in order:
                mixed_copy(level, slot, third).wait_send()

        @pl.when(s < n_sp - 1)
        def _():
            halo_copy(level).wait_send()

    own(0)
    own(1)
    prepare(0)
    for level in range(layers):
        first = 3 * level
        last = level == layers - 1
        if level == 0:
            hops(0)
            own(2)
            hops(1)
            if not last:
                own(3)
        crossed(first)
        crossed(first + 1)
        first_half(level)
        hops(first + 2)
        gating(level)
        if not last:
            hops(first + 3)
            own(first + 4)
        filtering(level)
        if not last:
            hops(first + 4)
            own(first + 5)
        relay(level, order[0])
        crossed(first + 2)
        for index in range(1, parts):
            relay(level, order[index])
            projecting(level, order[index - 1])
        projecting(level, order[-1])
        settle(level)
        if not last:
            prepare(level + 1)
    for phase in range(len(phases)):
        sent(phase)


def fused(n_sp, n_tp, *arrays):
    hidden_in, norm_gain, value_proj = arrays[:3]
    rows, feats = hidden_in.shape
    layers = norm_gain.shape[0]
    piece = value_proj.shape[2]
    blocks = n_sp // n_tp
    channels = blocks * piece
    kinds = 3
    vmem = pl.BlockSpec(memory_space=pltpu.VMEM)
    hbm = pl.BlockSpec(memory_space=pl.ANY)
    low, wide = jnp.bfloat16, jnp.float32
    slots = 2 + blocks + 3 * (rows // ROW_TILE) + 1
    return pl.pallas_call(
        lambda *refs: fused_kernel(n_sp, n_tp, *refs),
        out_shape=jax.ShapeDtypeStruct((rows, feats), low),
        in_specs=[vmem, vmem, hbm, hbm, vmem, vmem, vmem, vmem, hbm],
        out_specs=vmem,
        scratch_shapes=[
            pltpu.VMEM((layers, n_sp, feats, 2 * piece), low),
            pltpu.VMEM((layers, n_sp * piece, feats), low),
            pltpu.VMEM((rows, feats), low),
            pltpu.VMEM((n_tp, blocks, rows, 2 * piece), low),
            pltpu.VMEM((layers, 2, blocks, rows, 2 * piece), low),
            pltpu.VMEM((blocks, rows, 2 * piece), low),
            pltpu.VMEM((layers, blocks, rows, 2 * piece), low),
            pltpu.VMEM((HALO + rows, channels), wide),
            pltpu.VMEM((HALO, channels), low),
            pltpu.VMEM((layers, HALO, channels), low),
            pltpu.VMEM((layers, n_tp, rows, channels), low),
            pltpu.VMEM((layers, n_tp, 8, rows), wide),
            pltpu.SemaphoreType.DMA((layers, kinds)),
            pltpu.SemaphoreType.DMA((layers * kinds, 2, 3, n_sp)),
            pltpu.SemaphoreType.DMA((layers * kinds, 2, n_sp)),
            pltpu.SemaphoreType.DMA((layers, slots)),
            pltpu.SemaphoreType.DMA((layers, slots)),
            pltpu.SemaphoreType.DMA((layers, 3)),
            pltpu.SemaphoreType.DMA((layers, 3)),
        ],
        compiler_params=pltpu.CompilerParams(
            collective_id=0, has_side_effects=True, vmem_limit_bytes=VMEM_BYTES
        ),
    )(*arrays)


def solution(mesh):
    n_sp, n_tp = mesh.shape["sp"], mesh.shape["tp"]
    piece = C // n_sp
    small = n_tp == 4 and GROUPS == n_tp and n_sp % n_tp == 0 and piece % 128 == 0

    def local(*arrays):
        if small and arrays[0].shape[0] % ROW_TILE == 0:
            return fused(n_sp, n_tp, *arrays)
        return on_device(*arrays)

    return jax.shard_map(
        local,
        mesh=mesh,
        in_specs=(
            P("sp", "tp"),
            P(None, "tp"),
            P(None, "tp", "sp"),
            P(None, "tp", "sp"),
            P(None, None, "tp"),
            P(None, "tp"),
            P(None, "tp"),
            P(None, "tp"),
            P(None, "sp", "tp"),
        ),
        out_specs=P("sp", "tp"),
        check_vma=False,
    )
```

profile of v0, /device:TPU:0, one launch (start us, length us, event | category | flops | bytes accessed | tf_op | source)
XLA Modules:
  0.0 168.2 jit_solution(15629391575579319339)
XLA Ops:
  0.0 1.4 copy.10.refs_4_
  1.4 164.2 %shard_map.91 = bf16[768,1024]{1,0:T(8,128)(2,1)} custom-call(bf16[768,1024]{1,0:T(8,128)(2,1)} %refs_0_.1, bf16[2,1024]{1,0:T(2,128)(2,1)} %refs_1_.1, bf16[2,1024,128]{2,1,0:T(8,128)(2,1)} %refs_2_.1, bf16[2,1024,128]{2,1,0:T(8,128)(2,1)} %refs_3_.1, bf16[2,31,256]{2,1,0:T(8,128)(2,1)} %copy.10.refs_4_, bf16[2,256]{1,0:T(2,128)(2,1)} %refs_5_.1, ...), custom_call_target="tpu_custom_call" | custom-call | tf_op jit(solution)/shard_map/pallas_call | solution.py:543
  165.6 2.7 %copy.12 = bf16[768,1024]{1,0:T(8,128)(2,1)} copy(bf16[768,1024]{1,0:T(8,128)(2,1)} %shard_map.91) | data formatting | bytes 3145728
where the time goes:
time: 169 us; the launch traced here: 168 us
  Pallas kernels  164 us (97%)
  local copies, waits for them, and re-layouts  4.04 us (2%)
    pallas_call x1, Pallas kernels, fused(): pl.pallas_call(lambda *refs: fused_kernel(n_sp, n_tp, *refs), out_shape=j...  164 us
    unnamed x2, local copies, waits for them, and re-layouts  4.04 us

commit v1 on v0

v1 whole, which is shorter than its diff:
```python
import jax
import jax.numpy as jnp
from jax import lax
from jax.experimental import pallas as pl
from jax.experimental.pallas import tpu as pltpu
from jax.sharding import PartitionSpec as P

D = 4096
C = 1024
GROUPS = 4
WIDTH = 31


row_floor = 1e-06
group_floor = 1e-05


def passed_along(value, axis, steps):
    count = lax.axis_size(axis)
    initial, last = (max(0, -steps), min(count, count - steps))
    return lax.ppermute(value, axis, [(source, source + steps) for source in range(initial, last)])


def rms_normed(residual_rows, gain_part):
    wide_rows = residual_rows.astype(jnp.float32)
    squares = lax.psum(jnp.sum(wide_rows * wide_rows, axis=1), "tp")
    scale_rows = lax.rsqrt(squares / D + row_floor)
    return (wide_rows * scale_rows[:, None] * gain_part.astype(jnp.float32)[None, :]).astype(
        jnp.bfloat16
    )


def gated_input(normed_rows, w_value, w_gate):
    numbers = (((0,), (1,)), ((), ()))
    value_part = lax.dot_general(w_value, normed_rows, numbers, preferred_element_type=jnp.float32)
    gate_part = lax.dot_general(w_gate, normed_rows, numbers, preferred_element_type=jnp.float32)
    summed = lax.psum_scatter(
        jnp.stack([value_part, gate_part], axis=1).astype(jnp.bfloat16),
        "tp",
        scatter_dimension=0,
        tiled=True,
    ).astype(jnp.float32)
    return (summed[:, 0] * jax.nn.sigmoid(summed[:, 1])).astype(jnp.bfloat16)


def depthwise(extended, taps_part, bias_part, out_len):
    widened = extended.astype(jnp.float32)
    taps = taps_part.astype(jnp.float32)
    filtered = (
        jnp.zeros((extended.shape[0], out_len), jnp.float32)
        + bias_part.astype(jnp.float32)[:, None]
    )
    for offset in range(WIDTH):
        filtered = filtered + taps[offset][:, None] * widened[:, offset : offset + out_len]
    return filtered


def group_normed(filtered, gain_part, shift_part, group_size):
    channels, out_len = filtered.shape
    grouped = filtered.reshape(channels // group_size, group_size, out_len)
    group_mean = jnp.mean(grouped, axis=1, keepdims=True)
    centered = grouped - group_mean
    group_var = jnp.mean(centered * centered, axis=1, keepdims=True)
    scaled = (centered * lax.rsqrt(group_var + group_floor)).reshape(channels, out_len)
    scaled = (
        scaled * gain_part.astype(jnp.float32)[:, None] + shift_part.astype(jnp.float32)[:, None]
    )
    return jax.nn.silu(scaled).astype(jnp.bfloat16)


def project_out(mixed, w_out):
    return lax.dot_general(
        lax.all_gather(mixed, "tp", axis=0, tiled=True),
        w_out,
        (((0,), (0,)), ((), ())),
        preferred_element_type=jnp.float32,
    )


def on_device(
    hidden_in,
    norm_gain,
    value_proj,
    gate_proj,
    conv_taps,
    conv_bias,
    group_gain,
    group_shift,
    out_proj,
):
    tok_rows = hidden_in.shape[0]
    layers = norm_gain.shape[0]
    reach_back = WIDTH - 1
    group_size = C // GROUPS
    all_value, all_gate, all_out = (
        lax.all_gather(value_proj, "sp", axis=2, tiled=True),
        lax.all_gather(gate_proj, "sp", axis=2, tiled=True),
        lax.all_gather(out_proj, "sp", axis=1, tiled=True),
    )
    residual_rows = hidden_in
    for level in range(layers):
        w_value, w_gate, w_out = (all_value[level], all_gate[level], all_out[level])
        normed_rows = rms_normed(residual_rows, norm_gain[level])
        gated = gated_input(normed_rows, w_value, w_gate)
        before = passed_along(gated[:, tok_rows - reach_back :], "sp", 1)
        extended = jnp.concatenate([before, gated], axis=1)
        out_len = extended.shape[1] - reach_back
        filtered = depthwise(extended, conv_taps[level], conv_bias[level], out_len)
        mixed = group_normed(filtered, group_gain[level], group_shift[level], group_size)
        update = project_out(mixed, w_out)
        kept_rows = residual_rows
        residual_rows = (kept_rows.astype(jnp.float32) + update).astype(jnp.bfloat16)
    return residual_rows


MESH = pl.DeviceIdType.MESH
HALO = 32
ROW_TILE = 256
CONV_TILE = 64
VMEM_BYTES = 62 * 1024 * 1024


def fused_kernel(
    n_sp,
    n_tp,
    hidden_ref,
    norm_ref,
    value_ref,
    gate_ref,
    taps_ref,
    bias_ref,
    ggain_ref,
    gshift_ref,
    out_proj_ref,
    out_ref,
    w_in,
    w_out,
    scaled,
    part,
    from_core,
    to_chip,
    from_chip,
    taps,
    extended,
    halo_send,
    halo_recv,
    filtered,
    mixed,
    squares,
    scales,
    load_sem,
    w_send,
    w_recv,
    t_send,
    t_recv,
    s_send,
    s_recv,
):
    width, layers = taps_ref.shape[0], taps_ref.shape[1]
    rows, feats = hidden_ref.shape
    piece = value_ref.shape[2]
    blocks = n_sp // n_tp
    channels = blocks * piece
    reach = width - 1
    nz = n_sp // 2
    s = lax.axis_index("sp")
    t = lax.axis_index("tp")
    z, y = s // 2, s % 2
    chip, core = t // 2, t % 2
    core_mate = chip * 2 + (1 - core)
    chip_mate = (1 - chip) * 2 + core
    far_mate = (1 - chip) * 2 + (1 - core)
    across = z * 2 + 1 - y

    loads = []
    for level in range(layers):
        for kind, (source, target) in enumerate(
            (
                (value_ref.at[level], w_in.at[level, s, :, pl.ds(0, piece)]),
                (gate_ref.at[level], w_in.at[level, s, :, pl.ds(piece, piece)]),
                (
                    out_proj_ref.at[level],
                    w_out.at[level, pl.ds(pl.multiple_of(s * piece, piece), piece), :],
                ),
            )
        ):
            copy = pltpu.make_async_copy(source, target, load_sem.at[level, kind])
            copy.start()
            loads.append(copy)

    barrier = pltpu.get_barrier_semaphore()

    def greet(sp_index, tp_index):
        pl.semaphore_signal(barrier, inc=1, device_id=(sp_index, tp_index), device_id_type=MESH)

    up, down = z < nz - 1, z > 0
    corner_up = jnp.logical_and(up, y == 1)
    corner_down = jnp.logical_and(down, y == 0)
    for mate in (core_mate, chip_mate, far_mate):
        greet(s, mate)
    greet(across, t)
    for condition, target in (
        (up, s + 2),
        (down, s - 2),
        (corner_up, s + 1),
        (corner_down, s - 1),
    ):

        @pl.when(condition)
        def _(target=target):
            greet(target, t)

    mates = 4
    for condition in (up, down, corner_up, corner_down):
        mates = mates + condition.astype(jnp.int32)
    pl.semaphore_wait(barrier, mates)

    for copy in loads:
        copy.wait()

    phases = []
    for level in range(layers):
        phases += [("in", level), ("out", level)]

    def chunk(phase, owner, lot):
        kind, level = phases[phase]
        if kind == "in":
            size = feats // 2
            return w_in.at[level, owner, pl.ds(lot * size, size), :]
        size = piece // 2
        return w_out.at[
            level, pl.ds(pl.multiple_of(owner * piece + lot * size, size), size), :
        ]

    def weight_copy(phase, owner, way, lot):
        return pltpu.make_async_remote_copy(
            src_ref=chunk(phase, owner, lot),
            dst_ref=chunk(phase, owner, lot),
            send_sem=w_send.at[phase, lot, way, owner],
            recv_sem=w_recv.at[phase, lot, owner],
            device_id=((s + 2, s - 2, across)[way], t),
            device_id_type=MESH,
        )

    def go(phase, owner, way, lot, finish):
        copy = weight_copy(phase, owner, way, lot)
        if finish:
            copy.wait_send()
        else:
            copy.start()

    def come(phase, owner, lot, finish):
        if not finish:
            weight_copy(phase, owner, 2, lot).wait_recv()

    def own(phase, finish=False):
        for lot in (1, 0):
            go(phase, s, 2, lot, finish)
        for lot in (0, 1):
            for way, condition in enumerate((up, down)):

                @pl.when(condition)
                def _(way=way, lot=lot):
                    go(phase, s, way, lot, finish)

    def turn(phase, finish=False):
        for way, place in enumerate((0, nz - 1)):

            @pl.when(z == place)
            def _(way=way):
                come(phase, across, 1, finish)
                go(phase, across, way, 1, finish)

    def hop(phase, steps, finish=False):
        for lot in (0, 1):
            for way, sign in enumerate((-1, 1)):
                source = z + sign * steps
                inside = source >= 0 if way == 0 else source < nz
                inner = source > 0 if way == 0 else source < nz - 1
                onward = up if way == 0 else down

                @pl.when(inside)
                def _(way=way, lot=lot, source=source, inner=inner, onward=onward):
                    owner = source * 2 + y
                    come(phase, owner, lot, finish)

                    @pl.when(onward)
                    def _():
                        go(phase, owner, way, lot, finish)

                    if lot == 0:
                        go(phase, owner, 2, lot, finish)
                    else:

                        @pl.when(inner)
                        def _():
                            go(phase, owner, 2, lot, finish)

        for way, place in enumerate((0, nz - 1)):
            source = z - steps if way == 0 else z + steps
            onward = up if way == 0 else down

            @pl.when(source == place)
            def _(way=way, place=place, onward=onward):
                owner = place * 2 + 1 - y
                come(phase, owner, 1, finish)

                @pl.when(onward)
                def _():
                    go(phase, owner, way, 1, finish)

    def crossed(phase, source):
        owner = source * 2 + 1 - y
        come(phase, owner, 0, False)

        @pl.when(jnp.logical_and(source > 0, source < nz - 1))
        def _():
            come(phase, owner, 1, False)

    def sent(phase):
        own(phase, True)
        turn(phase, True)
        for steps in range(1, nz):
            hop(phase, steps, True)

    def tp_copy(level, slot, source, target, mate, sp_index=None):
        return pltpu.make_async_remote_copy(
            src_ref=source,
            dst_ref=target,
            send_sem=t_send.at[level, slot],
            recv_sem=t_recv.at[level, slot],
            device_id=(s if sp_index is None else sp_index, mate),
            device_id_type=MESH,
        )

    tiles = rows // ROW_TILE
    order = tuple(reversed(range(tiles)))

    def prepare(level, tile):
        gain = norm_ref[pl.ds(level, 1), :].astype(jnp.float32)
        ones = jnp.ones((8, feats), jnp.bfloat16)
        numbers = (((1,), (1,)), ((), ()))
        source = hidden_ref if level == 0 else out_ref
        span = pl.ds(tile * ROW_TILE, ROW_TILE)
        wide = source[span, :].astype(jnp.float32)
        scaled[span, :] = (wide * gain).astype(jnp.bfloat16)
        square = wide * wide
        high = square.astype(jnp.bfloat16)
        low = (square - high.astype(jnp.float32)).astype(jnp.bfloat16)
        total = lax.dot_general(ones, high, numbers, preferred_element_type=jnp.float32)
        total = total + lax.dot_general(ones, low, numbers, preferred_element_type=jnp.float32)
        squares[level, t, :, span] = total

    def square_copies(level):
        return [
            pltpu.make_async_remote_copy(
                src_ref=squares.at[level, t],
                dst_ref=squares.at[level, t],
                send_sem=s_send.at[level, slot],
                recv_sem=s_recv.at[level, slot],
                device_id=(s, mate),
                device_id_type=MESH,
            )
            for slot, mate in enumerate((core_mate, chip_mate, far_mate))
        ]

    def row_scales(level):
        for copy in square_copies(level):
            copy.wait_send()
            copy.wait_recv()
        total = squares[level, 0]
        for index in range(1, n_tp):
            total = total + squares[level, index]
        scales[...] = lax.rsqrt(total / D + row_floor).T

    def core_copy(level, target_chip, block):
        owner = target_chip * 2 + 1 - core
        return tp_copy(
            level,
            target_chip * blocks + block,
            part.at[owner, block],
            from_core.at[level, target_chip, block],
            core_mate,
        )

    base = 2 * blocks

    def chip_copy(level, block):
        return tp_copy(
            level, base + block, to_chip.at[block], from_chip.at[level, block], chip_mate
        )

    def halo_copy(level, block):
        return tp_copy(
            level,
            base + blocks + block,
            halo_send.at[block],
            halo_recv.at[level, block],
            t,
            s + 1,
        )

    def mixed_copy(level, slot, third):
        owner = (t, t, chip_mate)[slot]
        mate = (core_mate, chip_mate, core_mate)[slot]
        block = mixed.at[level, owner, pl.ds(third * ROW_TILE, ROW_TILE), :]
        return tp_copy(level, base + 2 * blocks + slot * tiles + third, block, block, mate)

    def target_of(turn_index):
        upper = z // (nz // 2)
        near = z + upper * (nz - 1 - 2 * z)
        pick = (near, 1 - near)[turn_index] if turn_index < 2 else turn_index
        return pick + upper * (nz - 1 - 2 * pick)

    def products(level, target, block):
        @pl.loop(0, tiles)
        def _(tile):
            span = pl.ds(pl.multiple_of(tile * ROW_TILE, ROW_TILE), ROW_TILE)
            part[target, block, span, :] = jnp.dot(
                scaled[span, :],
                w_in[level, target * blocks + block],
                preferred_element_type=jnp.float32,
            ).astype(jnp.bfloat16)

        @pl.when(target % 2 != core)
        def _():
            core_copy(level, target // 2, block).start()

    def contribute(level, target):
        products(level, target, y)
        crossed(2 * level, target)
        products(level, target, 1 - y)

    def pass_on(level, target):
        @pl.when(target == chip_mate)
        def _():
            for turn_index in range(blocks):
                block = (y + turn_index) % blocks
                core_copy(level, 1 - chip, block).wait_recv()

                @pl.loop(0, tiles)
                def _(tile, block=block):
                    span = pl.ds(pl.multiple_of(tile * ROW_TILE, ROW_TILE), ROW_TILE)
                    to_chip[block, span, :] = (
                        part[chip_mate, block, span, :].astype(jnp.float32)
                        + from_core[level, 1 - chip, block, span, :].astype(jnp.float32)
                    ).astype(jnp.bfloat16)

                chip_copy(level, block).start()

    def gating(level, block):
        core_copy(level, chip, block).wait_recv()
        chip_copy(level, block).wait_recv()

        @pl.loop(0, tiles)
        def _(tile):
            start = pl.multiple_of(tile * ROW_TILE, ROW_TILE)
            span = pl.ds(start, ROW_TILE)
            total = (
                part[t, block, span, :].astype(jnp.float32)
                + from_core[level, chip, block, span, :].astype(jnp.float32)
                + from_chip[level, block, span, :].astype(jnp.float32)
            ) * scales[span, 0:1]
            gated = (total[:, :piece] * jax.nn.sigmoid(total[:, piece:])).astype(jnp.bfloat16)
            extended[block, pl.ds(HALO + start, ROW_TILE), :] = gated.astype(jnp.float32)

        halo_send[block] = extended[block, pl.ds(rows, HALO), :].astype(jnp.bfloat16)

        @pl.when(s < n_sp - 1)
        def _():
            halo_copy(level, block).start()

    per_part = ROW_TILE // CONV_TILE

    def convolve(level, block, third):
        bias = taps[level, block, pl.ds(width, 1), :]
        weights = taps[level, block]

        @pl.loop(third * per_part, (third + 1) * per_part)
        def _(tile):
            start = pl.multiple_of(tile * CONV_TILE, CONV_TILE)
            window = extended[block, pl.ds(start, CONV_TILE + HALO), :]
            total = jnp.zeros((CONV_TILE, piece), jnp.float32) + bias
            for offset in range(width):
                low = HALO - reach + offset
                total = total + weights[offset : offset + 1, :] * window[low : low + CONV_TILE]
            filtered[block, pl.ds(start, CONV_TILE), :] = total

    def first_rows(level, block):
        @pl.when(s > 0)
        def _():
            halo_copy(level, block).wait_recv()
            extended[block, pl.ds(0, HALO), :] = halo_recv[level, block].astype(jnp.float32)

        @pl.when(s == 0)
        def _():
            extended[block, pl.ds(0, HALO), :] = jnp.zeros((HALO, piece), jnp.float32)

    def normalise(level, third):
        ggain = ggain_ref[pl.ds(level, 1), :].astype(jnp.float32)
        gshift = gshift_ref[pl.ds(level, 1), :].astype(jnp.float32)

        @pl.loop(third * per_part, (third + 1) * per_part)
        def _(tile):
            span = pl.ds(pl.multiple_of(tile * CONV_TILE, CONV_TILE), CONV_TILE)
            pieces = [filtered[block, span, :] for block in range(blocks)]
            mean = sum(jnp.sum(value, axis=1, keepdims=True) for value in pieces) / channels
            pieces = [value - mean for value in pieces]
            var = sum(jnp.sum(value * value, axis=1, keepdims=True) for value in pieces) / channels
            factor = lax.rsqrt(var + group_floor)
            for block in range(blocks):
                lanes = slice(block * piece, (block + 1) * piece)
                normed = pieces[block] * factor * ggain[:, lanes] + gshift[:, lanes]
                mixed[level, t, span, lanes] = (normed * jax.nn.sigmoid(normed)).astype(
                    jnp.bfloat16
                )

        mixed_copy(level, 1, third).start()
        mixed_copy(level, 0, third).start()

    def relay(level, third):
        mixed_copy(level, 1, third).wait_recv()
        mixed_copy(level, 2, third).start()

    def projecting(level, third):
        mixed_copy(level, 0, third).wait_recv()
        mixed_copy(level, 2, third).wait_recv()
        source = hidden_ref if level == 0 else out_ref
        span = pl.ds(third * ROW_TILE, ROW_TILE)
        total = source[span, :].astype(jnp.float32)
        for owner in range(n_tp):
            total = total + jnp.dot(
                mixed[level, owner, span, :],
                w_out[level, pl.ds(owner * channels, channels), :],
                preferred_element_type=jnp.float32,
            )
        out_ref[span, :] = total.astype(jnp.bfloat16)
        if level + 1 < layers:
            prepare(level + 1, third)

    def settle(level):
        for target_chip in range(2):
            for block in range(blocks):
                core_copy(level, target_chip, block).wait_send()
        for block in range(blocks):
            chip_copy(level, block).wait_send()
        for slot in range(3):
            for third in order:
                mixed_copy(level, slot, third).wait_send()

        @pl.when(s < n_sp - 1)
        def _():
            for block in range(blocks):
                halo_copy(level, block).wait_send()

    own(0)
    for level in range(layers):
        for block in range(blocks):
            lanes = slice(block * piece, (block + 1) * piece)
            taps[level, block, 0:width, :] = taps_ref[:, level, lanes].astype(jnp.float32)
            taps[level, block, width : width + 1, :] = bias_ref[level : level + 1, lanes].astype(
                jnp.float32
            )
    for tile in range(tiles):
        prepare(0, tile)
    for copy in square_copies(0):
        copy.start()
    turn(0)
    for level in range(layers):
        first, second = 2 * level, 2 * level + 1
        last = level == layers - 1
        targets = [target_of(turn_index) for turn_index in range(n_tp)]
        hop(first, 1)
        contribute(level, targets[0])
        hop(first, 2)
        own(second)
        pass_on(level, targets[0])
        contribute(level, targets[1])
        turn(second)
        pass_on(level, targets[1])
        hop(first, 3)
        contribute(level, targets[2])
        pass_on(level, targets[2])
        contribute(level, targets[3])
        pass_on(level, targets[3])
        hop(second, 1)
        row_scales(level)
        gating(level, y)
        for third in order[:-1]:
            convolve(level, y, third)
        hop(second, 2)
        if not last:
            own(first + 2)
        gating(level, 1 - y)
        for third in order[:-1]:
            convolve(level, 1 - y, third)
            normalise(level, third)
        if not last:
            turn(first + 2)
        for block in (y, 1 - y):
            first_rows(level, block)
            convolve(level, block, order[-1])
        normalise(level, order[-1])
        hop(second, 3)
        relay(level, order[0])
        for source in range(nz):
            crossed(second, source)
        for index in range(1, tiles):
            relay(level, order[index])
            projecting(level, order[index - 1])
        projecting(level, order[-1])
        if not last:
            for copy in square_copies(level + 1):
                copy.start()
        settle(level)
    for phase in range(len(phases)):
        sent(phase)


def fused(n_sp, n_tp, *arrays):
    hidden_in, norm_gain, value_proj = arrays[:3]
    rows, feats = hidden_in.shape
    layers = norm_gain.shape[0]
    piece = value_proj.shape[2]
    blocks = n_sp // n_tp
    channels = blocks * piece
    kinds = 3
    vmem = pl.BlockSpec(memory_space=pltpu.VMEM)
    hbm = pl.BlockSpec(memory_space=pl.ANY)
    low, wide = jnp.bfloat16, jnp.float32
    slots = 4 * blocks + 3 * (rows // ROW_TILE)
    arrays = arrays[:4] + (arrays[4].transpose(1, 0, 2),) + arrays[5:]
    return pl.pallas_call(
        lambda *refs: fused_kernel(n_sp, n_tp, *refs),
        out_shape=jax.ShapeDtypeStruct((rows, feats), low),
        in_specs=[vmem, vmem, hbm, hbm, vmem, vmem, vmem, vmem, hbm],
        out_specs=vmem,
        scratch_shapes=[
            pltpu.VMEM((layers, n_sp, feats, 2 * piece), low),
            pltpu.VMEM((layers, n_sp * piece, feats), low),
            pltpu.VMEM((rows, feats), low),
            pltpu.VMEM((n_tp, blocks, rows, 2 * piece), low),
            pltpu.VMEM((layers, 2, blocks, rows, 2 * piece), low),
            pltpu.VMEM((blocks, rows, 2 * piece), low),
            pltpu.VMEM((layers, blocks, rows, 2 * piece), low),
            pltpu.VMEM((layers, blocks, WIDTH + 1, piece), wide),
            pltpu.VMEM((blocks, HALO + rows, piece), wide),
            pltpu.VMEM((blocks, HALO, piece), low),
            pltpu.VMEM((layers, blocks, HALO, piece), low),
            pltpu.VMEM((blocks, rows, piece), wide),
            pltpu.VMEM((layers, n_tp, rows, channels), low),
            pltpu.VMEM((layers, n_tp, 8, rows), wide),
            pltpu.VMEM((rows, 8), wide),
            pltpu.SemaphoreType.DMA((layers, kinds)),
            pltpu.SemaphoreType.DMA((layers * 2, 2, 3, n_sp)),
            pltpu.SemaphoreType.DMA((layers * 2, 2, n_sp)),
            pltpu.SemaphoreType.DMA((layers, slots)),
            pltpu.SemaphoreType.DMA((layers, slots)),
            pltpu.SemaphoreType.DMA((layers, 3)),
            pltpu.SemaphoreType.DMA((layers, 3)),
        ],
        compiler_params=pltpu.CompilerParams(
            collective_id=0, has_side_effects=True, vmem_limit_bytes=VMEM_BYTES
        ),
    )(*arrays)


def solution(mesh):
    n_sp, n_tp = mesh.shape["sp"], mesh.shape["tp"]
    piece = C // n_sp
    small = n_tp == 4 and GROUPS == n_tp and n_sp == 2 * n_tp and piece % 128 == 0

    def local(*arrays):
        if small and arrays[0].shape[0] % ROW_TILE == 0:
            return fused(n_sp, n_tp, *arrays)
        return on_device(*arrays)

    return jax.shard_map(
        local,
        mesh=mesh,
        in_specs=(
            P("sp", "tp"),
            P(None, "tp"),
            P(None, "tp", "sp"),
            P(None, "tp", "sp"),
            P(None, None, "tp"),
            P(None, "tp"),
            P(None, "tp"),
            P(None, "tp"),
            P(None, "sp", "tp"),
        ),
        out_specs=P("sp", "tp"),
        check_vma=False,
    )
```

time: 169 us -> 160 us (0.947)
  Pallas kernels: 164 us -> 157 us
    pallas_call x1, Pallas kernels: 164 us -> 157 us  [fused(): pl.pallas_call(lambda *refs: fused_kernel(n_sp, n_tp, *refs), out_shape=j...]
    unnamed x2 -> x1, local copies, waits for them, and re-layouts: 4.04 us -> 2.67 us
where the time goes in v1:
time: 160 us; the launch traced here: 159 us
  Pallas kernels  157 us (98%)
  local copies, waits for them, and re-layouts  2.67 us (2%)
    pallas_call x1, Pallas kernels, fused(): pl.pallas_call(lambda *refs: fused_kernel(n_sp, n_tp, *refs), out_shape=j...  157 us

profile of v1, /device:TPU:0, one launch (start us, length us, event | category | flops | bytes accessed | tf_op | source)
XLA Modules:
  0.0 159.5 jit_solution(10048332736483402172)
XLA Ops:
  0.0 156.8 %shard_map.91 = bf16[768,1024]{1,0:T(8,128)(2,1)} custom-call(bf16[768,1024]{1,0:T(8,128)(2,1)} %refs_0_.1, bf16[2,1024]{1,0:T(2,128)(2,1)} %refs_1_.1, bf16[2,1024,128]{2,1,0:T(8,128)(2,1)} %refs_2_.1, bf16[2,1024,128]{2,1,0:T(8,128)(2,1)} %refs_3_.1, bf16[31,2,256]{2,1,0:T(2,128)(2,1)} %bitcast.1, bf16[2,256]{1,0:T(2,128)(2,1)} %refs_5_.1, ...), custom_call_target="tpu_custom_call" | custom-call | tf_op jit(solution)/shard_map/pallas_call | solution.py:633
  156.8 2.7 %copy.11 = bf16[768,1024]{1,0:T(8,128)(2,1)} copy(bf16[768,1024]{1,0:T(8,128)(2,1)} %shard_map.91) | data formatting | bytes 3145728

commit v2 on v1

--- a/solution.py
+++ b/solution.py
@@ -253,9 +253,14 @@
         if not finish:
             weight_copy(phase, owner, 2, lot).wait_recv()
 
-    def own(phase, finish=False):
+    outer = jnp.logical_or(z == 0, z == nz - 1)
+    middle = jnp.logical_and(z > 0, z < nz - 1)
+
+    def own_rows(phase, finish=False):
         for lot in (1, 0):
             go(phase, s, 2, lot, finish)
+
+    def own_column(phase, finish=False):
         for lot in (0, 1):
             for way, condition in enumerate((up, down)):
 
@@ -271,8 +276,8 @@
                 come(phase, across, 1, finish)
                 go(phase, across, way, 1, finish)
 
-    def hop(phase, steps, finish=False):
-        for lot in (0, 1):
+    def hop(phase, steps, lots=(0, 1), finish=False):
+        for lot in lots:
             for way, sign in enumerate((-1, 1)):
                 source = z + sign * steps
                 inside = source >= 0 if way == 0 else source < nz
@@ -296,6 +301,7 @@
                         def _():
                             go(phase, owner, 2, lot, finish)
 
+    def side(phase, steps, finish=False):
         for way, place in enumerate((0, nz - 1)):
             source = z - steps if way == 0 else z + steps
             onward = up if way == 0 else down
@@ -309,6 +315,12 @@
                 def _():
                     go(phase, owner, way, 1, finish)
 
+    def apart(condition, *steps):
+        @pl.when(condition)
+        def _():
+            for function, *arguments in steps:
+                function(*arguments)
+
     def crossed(phase, source):
         owner = source * 2 + 1 - y
         come(phase, owner, 0, False)
@@ -318,10 +330,12 @@
             come(phase, owner, 1, False)
 
     def sent(phase):
-        own(phase, True)
+        own_rows(phase, True)
+        own_column(phase, True)
         turn(phase, True)
         for steps in range(1, nz):
-            hop(phase, steps, True)
+            hop(phase, steps, finish=True)
+            side(phase, steps, True)
 
     def tp_copy(level, slot, source, target, mate, sp_index=None):
         return pltpu.make_async_remote_copy(
@@ -426,27 +440,28 @@
         def _():
             core_copy(level, target // 2, block).start()
 
-    def contribute(level, target):
-        products(level, target, y)
-        crossed(2 * level, target)
-        products(level, target, 1 - y)
-
-    def pass_on(level, target):
+    def contribute(level, target, turned):
+        block = 1 - y if turned else y
+        if turned:
+            crossed(2 * level, target)
+        products(level, target, block)
+
+    def pass_on(level, target, turned):
+        block = 1 - y if turned else y
+
         @pl.when(target == chip_mate)
         def _():
-            for turn_index in range(blocks):
-                block = (y + turn_index) % blocks
-                core_copy(level, 1 - chip, block).wait_recv()
-
-                @pl.loop(0, tiles)
-                def _(tile, block=block):
-                    span = pl.ds(pl.multiple_of(tile * ROW_TILE, ROW_TILE), ROW_TILE)
-                    to_chip[block, span, :] = (
-                        part[chip_mate, block, span, :].astype(jnp.float32)
-                        + from_core[level, 1 - chip, block, span, :].astype(jnp.float32)
-                    ).astype(jnp.bfloat16)
-
-                chip_copy(level, block).start()
+            core_copy(level, 1 - chip, block).wait_recv()
+
+            @pl.loop(0, tiles)
+            def _(tile):
+                span = pl.ds(pl.multiple_of(tile * ROW_TILE, ROW_TILE), ROW_TILE)
+                to_chip[block, span, :] = (
+                    part[chip_mate, block, span, :].astype(jnp.float32)
+                    + from_core[level, 1 - chip, block, span, :].astype(jnp.float32)
+                ).astype(jnp.bfloat16)
+
+            chip_copy(level, block).start()
 
     def gating(level, block):
         core_copy(level, chip, block).wait_recv()
@@ -553,7 +568,8 @@
             for block in range(blocks):
                 halo_copy(level, block).wait_send()
 
-    own(0)
+    own_rows(0)
+    own_column(0)
     for level in range(layers):
         for block in range(blocks):
             lanes = slice(block * piece, (block + 1) * piece)
@@ -565,53 +581,85 @@
         prepare(0, tile)
     for copy in square_copies(0):
         copy.start()
-    turn(0)
+    apart(outer, (turn, 0), *((own_column, phase) for phase in range(1, len(phases))))
+    end = outer.astype(jnp.int32)
     for level in range(layers):
         first, second = 2 * level, 2 * level + 1
         last = level == layers - 1
         targets = [target_of(turn_index) for turn_index in range(n_tp)]
-        hop(first, 1)
-        contribute(level, targets[0])
-        hop(first, 2)
-        own(second)
-        pass_on(level, targets[0])
-        contribute(level, targets[1])
-        turn(second)
-        pass_on(level, targets[1])
-        hop(first, 3)
-        contribute(level, targets[2])
-        pass_on(level, targets[2])
-        contribute(level, targets[3])
-        pass_on(level, targets[3])
-        hop(second, 1)
+        third_target = targets[2] * end + targets[3] * (1 - end)
+        contribute(level, targets[0], 0)
+        if level == 0:
+            hop(first, 1)
+        else:
+            apart(outer, (turn, first), (hop, first, 1, (1,)))
+        contribute(level, targets[1], 0)
+        apart(middle, (contribute, level, targets[2], 0))
+        contribute(level, targets[0], 1)
+        pass_on(level, targets[0], 0)
+        apart(middle, (side, first, 1))
+        if level == 0:
+            hop(first, 2)
+        else:
+            apart(outer, (hop, first, 2))
+        pass_on(level, targets[1], 0)
+        apart(middle, (pass_on, level, targets[2], 0))
+        contribute(level, third_target, 0)
+        pass_on(level, targets[0], 1)
+        contribute(level, targets[1], 1)
+        apart(
+            outer,
+            (hop, first, 3),
+            (own_rows, second),
+            (contribute, level, targets[3], 0),
+        )
+        pass_on(level, third_target, 0)
+        pass_on(level, targets[1], 1)
+        contribute(level, targets[2], 1)
+        apart(outer, (pass_on, level, targets[3], 0))
+        pass_on(level, targets[2], 1)
+        apart(outer, (side, first, nz - 1))
+        apart(middle, (side, first, nz - 2), (own_rows, second), (own_column, second))
+        contribute(level, targets[3], 1)
+        pass_on(level, targets[3], 1)
+        apart(outer, (turn, second), (hop, second, 1), (hop, second, 2, (0,)))
+        apart(middle, (hop, second, 1))
         row_scales(level)
         gating(level, y)
         for third in order[:-1]:
             convolve(level, y, third)
-        hop(second, 2)
-        if not last:
-            own(first + 2)
+        apart(outer, (hop, second, 2, (1,)))
         gating(level, 1 - y)
+        apart(middle, (hop, second, 2))
         for third in order[:-1]:
             convolve(level, 1 - y, third)
             normalise(level, third)
+            if third == order[0]:
+                apart(outer, (hop, second, 3, (0,)))
+                if not last:
+                    apart(outer, (own_rows, first + 2))
+        apart(middle, (side, second, 1), (side, second, 2))
         if not last:
-            turn(first + 2)
+            apart(middle, (own_rows, first + 2), (own_column, first + 2))
         for block in (y, 1 - y):
             first_rows(level, block)
             convolve(level, block, order[-1])
         normalise(level, order[-1])
-        hop(second, 3)
         relay(level, order[0])
+        apart(outer, (hop, second, 3, (1,)), (side, second, nz - 1))
         for source in range(nz):
             crossed(second, source)
         for index in range(1, tiles):
             relay(level, order[index])
             projecting(level, order[index - 1])
+        if not last:
+            apart(middle, (hop, first + 2, 1))
+            apart(outer, (hop, first + 2, 1, (0,)))
         projecting(level, order[-1])
         if not last:
             for copy in square_copies(level + 1):
                 copy.start()
+            apart(middle, (hop, first + 2, 2))
         settle(level)
     for phase in range(len(phases)):
         sent(phase)

time: 160 us -> 141 us (0.88)
  Pallas kernels: 157 us -> 139 us
    pallas_call x1, Pallas kernels: 157 us -> 139 us  [fused(): pl.pallas_call(lambda *refs: fused_kernel(n_sp, n_tp, *refs), out_shape=j...]
where the time goes in v2:
time: 141 us
  Pallas kernels  139 us (99%)
  local copies, waits for them, and re-layouts  2.67 us (2%)
    pallas_call x1, Pallas kernels, fused(): pl.pallas_call(lambda *refs: fused_kernel(n_sp, n_tp, *refs), out_shape=j...  139 us

profile of v2, /device:TPU:0, one launch (start us, length us, event | category | flops | bytes accessed | tf_op | source)
XLA Modules:
  0.0 141.2 jit_solution(1093276427953881134)
XLA Ops:
  0.0 138.5 %shard_map.91 = bf16[768,1024]{1,0:T(8,128)(2,1)} custom-call(bf16[768,1024]{1,0:T(8,128)(2,1)} %refs_0_.1, bf16[2,1024]{1,0:T(2,128)(2,1)} %refs_1_.1, bf16[2,1024,128]{2,1,0:T(8,128)(2,1)} %refs_2_.1, bf16[2,1024,128]{2,1,0:T(8,128)(2,1)} %refs_3_.1, bf16[31,2,256]{2,1,0:T(2,128)(2,1)} %bitcast.1, bf16[2,256]{1,0:T(2,128)(2,1)} %refs_5_.1, ...), custom_call_target="tpu_custom_call" | custom-call | tf_op jit(solution)/shard_map/pallas_call | solution.py:681
  138.5 2.7 %copy.11 = bf16[768,1024]{1,0:T(8,128)(2,1)} copy(bf16[768,1024]{1,0:T(8,128)(2,1)} %shard_map.91) | data formatting | bytes 3145728

commit v3 on v2

--- a/solution.py
+++ b/solution.py
@@ -133,6 +133,7 @@
     gshift_ref,
     out_proj_ref,
     out_ref,
+    held,
     w_in,
     w_out,
     scaled,
@@ -148,13 +149,26 @@
     mixed,
     squares,
     scales,
+    guest,
+    guest_part,
+    guest_core,
+    guest_out,
+    guest_in,
+    guest_gated,
+    lent,
+    guest_sum,
+    guest_sums,
+    guest_scales,
     load_sem,
+    result_sem,
     w_send,
     w_recv,
     t_send,
     t_recv,
     s_send,
     s_recv,
+    g_send,
+    g_recv,
 ):
     width, layers = taps_ref.shape[0], taps_ref.shape[1]
     rows, feats = hidden_ref.shape
@@ -172,6 +186,7 @@
     far_mate = (1 - chip) * 2 + (1 - core)
     across = z * 2 + 1 - y
 
+    taken = pltpu.make_async_copy(hidden_ref, held, load_sem.at[0, 3])
     loads = []
     for level in range(layers):
         for kind, (source, target) in enumerate(
@@ -188,6 +203,7 @@
             copy.start()
             loads.append(copy)
 
+    taken.start()
     barrier = pltpu.get_barrier_semaphore()
 
     def greet(sp_index, tp_index):
@@ -215,7 +231,7 @@
         mates = mates + condition.astype(jnp.int32)
     pl.semaphore_wait(barrier, mates)
 
-    for copy in loads:
+    for copy in loads[:2]:
         copy.wait()
 
     phases = []
@@ -232,11 +248,19 @@
             level, pl.ds(pl.multiple_of(owner * piece + lot * size, size), size), :
         ]
 
+    def place_of(owner, way, lot):
+        source, column = owner // 2, owner % 2
+        if way == 2:
+            return 2 * source + lot
+        return 2 * nz + (2 * (source + way) + lot) * (1 - (column + y) % 2) + (
+            2 * (nz + 1) + way
+        ) * ((column + y) % 2)
+
     def weight_copy(phase, owner, way, lot):
         return pltpu.make_async_remote_copy(
             src_ref=chunk(phase, owner, lot),
             dst_ref=chunk(phase, owner, lot),
-            send_sem=w_send.at[phase, lot, way, owner],
+            send_sem=w_send.at[phase, place_of(owner, way, lot)],
             recv_sem=w_recv.at[phase, lot, owner],
             device_id=((s + 2, s - 2, across)[way], t),
             device_id_type=MESH,
@@ -260,9 +284,12 @@
         for lot in (1, 0):
             go(phase, s, 2, lot, finish)
 
-    def own_column(phase, finish=False):
+    def own_column(phase, ends=None, finish=False):
+        to_end = (z == nz - 2, z == 1)
+        to_middle = (z < nz - 2, z > 1)
+        conditions = (up, down) if ends is None else to_end if ends else to_middle
         for lot in (0, 1):
-            for way, condition in enumerate((up, down)):
+            for way, condition in enumerate(conditions):
 
                 @pl.when(condition)
                 def _(way=way, lot=lot):
@@ -276,13 +303,20 @@
                 come(phase, across, 1, finish)
                 go(phase, across, way, 1, finish)
 
-    def hop(phase, steps, lots=(0, 1), finish=False):
+    def hop(phase, steps, lots=(0, 1), ends=None, finish=False):
         for lot in lots:
             for way, sign in enumerate((-1, 1)):
                 source = z + sign * steps
                 inside = source >= 0 if way == 0 else source < nz
                 inner = source > 0 if way == 0 else source < nz - 1
                 onward = up if way == 0 else down
+                if phase == 0:
+                    onward = z < nz - 2 if way == 0 else z > 1
+                    if steps > 1:
+                        inside = jnp.logical_and(inside, middle)
+                if ends is not None:
+                    place = 0 if way == 0 else nz - 1
+                    inside = source == place if ends else jnp.logical_and(inside, inner)
 
                 @pl.when(inside)
                 def _(way=way, lot=lot, source=source, inner=inner, onward=onward):
@@ -302,9 +336,13 @@
                             go(phase, owner, 2, lot, finish)
 
     def side(phase, steps, finish=False):
+        if phase == 0 and steps == nz - 1:
+            return
         for way, place in enumerate((0, nz - 1)):
             source = z - steps if way == 0 else z + steps
             onward = up if way == 0 else down
+            if phase == 0:
+                onward = z < nz - 2 if way == 0 else z > 1
 
             @pl.when(source == place)
             def _(way=way, place=place, onward=onward):
@@ -331,18 +369,18 @@
 
     def sent(phase):
         own_rows(phase, True)
-        own_column(phase, True)
+        own_column(phase, finish=True)
         turn(phase, True)
         for steps in range(1, nz):
             hop(phase, steps, finish=True)
-            side(phase, steps, True)
+            side(phase, steps, finish=True)
 
     def tp_copy(level, slot, source, target, mate, sp_index=None):
         return pltpu.make_async_remote_copy(
             src_ref=source,
             dst_ref=target,
-            send_sem=t_send.at[level, slot],
-            recv_sem=t_recv.at[level, slot],
+            send_sem=t_send.at[slot],
+            recv_sem=t_recv.at[slot],
             device_id=(s if sp_index is None else sp_index, mate),
             device_id_type=MESH,
         )
@@ -354,9 +392,8 @@
         gain = norm_ref[pl.ds(level, 1), :].astype(jnp.float32)
         ones = jnp.ones((8, feats), jnp.bfloat16)
         numbers = (((1,), (1,)), ((), ()))
-        source = hidden_ref if level == 0 else out_ref
         span = pl.ds(tile * ROW_TILE, ROW_TILE)
-        wide = source[span, :].astype(jnp.float32)
+        wide = held[span, :].astype(jnp.float32)
         scaled[span, :] = (wide * gain).astype(jnp.bfloat16)
         square = wide * wide
         high = square.astype(jnp.bfloat16)
@@ -370,8 +407,8 @@
             pltpu.make_async_remote_copy(
                 src_ref=squares.at[level, t],
                 dst_ref=squares.at[level, t],
-                send_sem=s_send.at[level, slot],
-                recv_sem=s_recv.at[level, slot],
+                send_sem=s_send.at[slot],
+                recv_sem=s_recv.at[slot],
                 device_id=(s, mate),
                 device_id_type=MESH,
             )
@@ -386,6 +423,8 @@
         for index in range(1, n_tp):
             total = total + squares[level, index]
         scales[...] = lax.rsqrt(total / D + row_floor).T
+        if level == 0:
+            guest_sum[...] = total
 
     def core_copy(level, target_chip, block):
         owner = target_chip * 2 + 1 - core
@@ -407,7 +446,7 @@
     def halo_copy(level, block):
         return tp_copy(
             level,
-            base + blocks + block,
+            base + (1 + level) * blocks + block,
             halo_send.at[block],
             halo_recv.at[level, block],
             t,
@@ -418,7 +457,7 @@
         owner = (t, t, chip_mate)[slot]
         mate = (core_mate, chip_mate, core_mate)[slot]
         block = mixed.at[level, owner, pl.ds(third * ROW_TILE, ROW_TILE), :]
-        return tp_copy(level, base + 2 * blocks + slot * tiles + third, block, block, mate)
+        return tp_copy(level, base + (1 + layers) * blocks + slot * tiles + third, block, block, mate)
 
     def target_of(turn_index):
         upper = z // (nz // 2)
@@ -484,6 +523,109 @@
         @pl.when(s < n_sp - 1)
         def _():
             halo_copy(level, block).start()
+
+    upper_half = z // (nz // 2)
+    guest_chip = 1 - upper_half
+    host = jnp.logical_and(middle, chip == guest_chip)
+    feeder = jnp.logical_and(middle, chip != guest_chip)
+    lender = jnp.logical_and(outer, chip == guest_chip)
+    keeper = jnp.logical_and(outer, chip != guest_chip)
+
+    def guest_copy(kind, third):
+        span = pl.ds(third * ROW_TILE, ROW_TILE)
+        inward = s + 2 - 4 * upper_half
+        outward = s - 2 + 4 * upper_half
+        source, target, place, mate = (
+            (scaled.at[span, :], guest.at[span, :], inward, t),
+            (guest_part.at[1, third], guest_core.at[third], s, core_mate),
+            (guest_out.at[third], guest_in.at[third], s, chip_mate),
+            (guest_gated.at[third], lent.at[third], outward, t),
+            (guest_sum, guest_sums, inward, t),
+        )[kind]
+        return pltpu.make_async_remote_copy(
+            src_ref=source,
+            dst_ref=target,
+            send_sem=g_send.at[kind * tiles + third],
+            recv_sem=g_recv.at[kind * tiles + third],
+            device_id=(place, mate),
+            device_id_type=MESH,
+        )
+
+    def guest_start():
+        guest_copy(4, 0).start()
+        for third in order[:-1]:
+            guest_copy(0, third).start()
+        own_column(1)
+        guest_copy(0, order[-1]).start()
+
+    def guest_left():
+        guest_copy(4, 0).wait_send()
+        for third in order:
+            guest_copy(0, third).wait_send()
+
+    def guest_scale():
+        guest_copy(4, 0).wait_recv()
+        guest_scales[...] = lax.rsqrt(guest_sums[...] / D + row_floor).T
+
+    def guest_products(third):
+        guest_copy(0, third).wait_recv()
+        span = pl.ds(third * ROW_TILE, ROW_TILE)
+
+        for which in (1, 0):
+            owner = (guest_chip * 2 + (core if which == 0 else 1 - core)) * blocks
+
+            @pl.loop(0, blocks)
+            def _(block, which=which, owner=owner):
+                guest_part[which, third, block] = jnp.dot(
+                    guest[span, :], w_in[0, owner + block], preferred_element_type=jnp.float32
+                ).astype(jnp.bfloat16)
+
+            if which == 1:
+                guest_copy(1, third).start()
+
+    def guest_pass(third):
+        guest_copy(1, third).wait_recv()
+        guest_out[third] = (
+            guest_part[0, third].astype(jnp.float32) + guest_core[third].astype(jnp.float32)
+        ).astype(jnp.bfloat16)
+        guest_copy(2, third).start()
+
+    def guest_gate(third):
+        guest_copy(1, third).wait_recv()
+        guest_copy(2, third).wait_recv()
+        span = pl.ds(third * ROW_TILE, ROW_TILE)
+        for block in range(blocks):
+            total = (
+                guest_part[0, third, block].astype(jnp.float32)
+                + guest_core[third, block].astype(jnp.float32)
+                + guest_in[third, block].astype(jnp.float32)
+            ) * guest_scales[span, 0:1]
+            guest_gated[third, block] = (
+                total[:, :piece] * jax.nn.sigmoid(total[:, piece:])
+            ).astype(jnp.bfloat16)
+        guest_copy(3, third).start()
+
+    def lend(third):
+        guest_copy(3, third).wait_recv()
+        for block in range(blocks):
+            extended[block, pl.ds(HALO + third * ROW_TILE, ROW_TILE), :] = lent[
+                third, block
+            ].astype(jnp.float32)
+            if third == tiles - 1:
+                halo_send[block] = lent[third, block, ROW_TILE - HALO :, :]
+
+                @pl.when(s < n_sp - 1)
+                def _(block=block):
+                    halo_copy(0, block).start()
+
+    def guest_settle():
+        for third in order:
+            apart(middle, (guest_sent, 1, third))
+            apart(feeder, (guest_sent, 2, third))
+            apart(host, (guest_sent, 3, third))
+
+    def guest_sent(kind, third):
+        guest_copy(kind, third).wait_send()
 
     per_part = ROW_TILE // CONV_TILE
 
@@ -540,25 +682,40 @@
     def projecting(level, third):
         mixed_copy(level, 0, third).wait_recv()
         mixed_copy(level, 2, third).wait_recv()
-        source = hidden_ref if level == 0 else out_ref
         span = pl.ds(third * ROW_TILE, ROW_TILE)
-        total = source[span, :].astype(jnp.float32)
+        total = held[span, :].astype(jnp.float32)
         for owner in range(n_tp):
             total = total + jnp.dot(
                 mixed[level, owner, span, :],
                 w_out[level, pl.ds(owner * channels, channels), :],
                 preferred_element_type=jnp.float32,
             )
-        out_ref[span, :] = total.astype(jnp.bfloat16)
+        held[span, :] = total.astype(jnp.bfloat16)
         if level + 1 < layers:
             prepare(level + 1, third)
+        else:
+            result_copy(third).start()
+
+    def result_copy(third):
+        span = pl.ds(third * ROW_TILE, ROW_TILE)
+        return pltpu.make_async_copy(held.at[span, :], out_ref.at[span, :], result_sem.at[third])
 
     def settle(level):
         for target_chip in range(2):
+            used = middle if level == 0 else z >= 0
+
+            @pl.when(jnp.logical_or(used, target_chip != guest_chip))
+            def _(target_chip=target_chip):
+                for block in range(blocks):
+                    core_copy(level, target_chip, block).wait_send()
+
+        passed = jnp.logical_or(middle, lender) if level == 0 else z >= 0
+
+        @pl.when(passed)
+        def _():
             for block in range(blocks):
-                core_copy(level, target_chip, block).wait_send()
-        for block in range(blocks):
-            chip_copy(level, block).wait_send()
+                chip_copy(level, block).wait_send()
+
         for slot in range(3):
             for third in order:
                 mixed_copy(level, slot, third).wait_send()
@@ -570,6 +727,8 @@
 
     own_rows(0)
     own_column(0)
+    for copy in loads[2:]:
+        copy.wait()
     for level in range(layers):
         for block in range(blocks):
             lanes = slice(block * piece, (block + 1) * piece)
@@ -577,92 +736,192 @@
             taps[level, block, width : width + 1, :] = bias_ref[level : level + 1, lanes].astype(
                 jnp.float32
             )
+    taken.wait()
     for tile in range(tiles):
         prepare(0, tile)
     for copy in square_copies(0):
         copy.start()
-    apart(outer, (turn, 0), *((own_column, phase) for phase in range(1, len(phases))))
+    row_scales(0)
+    goals = [target_of(turn_index) for turn_index in range(n_tp)]
+
+    def late(third):
+        for block in (y, 1 - y):
+            convolve(0, block, third)
+        normalise(0, third)
+
+    def end_start():
+        turn(0)
+        guest_start()
+        contribute(0, goals[0], 0)
+        hop(0, 1)
+        own_rows(1)
+        contribute(0, goals[1], 0)
+        contribute(0, goals[0], 1)
+        pass_on(0, goals[0], 0)
+        pass_on(0, goals[1], 0)
+        contribute(0, goals[1], 1)
+        pass_on(0, goals[0], 1)
+        pass_on(0, goals[1], 1)
+        turn(1)
+        hop(1, 1)
+        own_rows(2)
+        apart(
+            keeper,
+            (gating, 0, y),
+            (gating, 0, 1 - y),
+        )
+        hop(1, 2)
+        hop(2, 1)
+        apart(
+            keeper,
+            *((convolve, 0, y, third) for third in order[:-1]),
+            *(
+                step
+                for third in order[:-1]
+                for step in ((convolve, 0, 1 - y, third), (normalise, 0, third))
+            ),
+        )
+        apart(lender, (lend, order[0]))
+        own_column(2)
+        turn(2)
+        apart(lender, (lend, order[1]), (late, order[0]))
+        hop(1, 3)
+        own_column(3)
+        apart(lender, (lend, order[2]), (late, order[1]))
+        hop(2, 2, (0,))
+
+    def middle_start():
+        for phase in range(1, len(phases)):
+            own_column(phase, True)
+        contribute(0, goals[0], 0)
+        hop(0, 1)
+        contribute(0, goals[1], 0)
+        contribute(0, goals[2], 0)
+        contribute(0, goals[0], 1)
+        pass_on(0, goals[0], 0)
+        side(0, 1)
+        hop(0, 2)
+        own_rows(1)
+        own_column(1, False)
+        pass_on(0, goals[1], 0)
+        pass_on(0, goals[2], 0)
+        contribute(0, goals[3], 0)
+        pass_on(0, goals[0], 1)
+        contribute(0, goals[1], 1)
+        pass_on(0, goals[3], 0)
+        pass_on(0, goals[1], 1)
+        contribute(0, goals[2], 1)
+        side(0, 2)
+        pass_on(0, goals[2], 1)
+        contribute(0, goals[3], 1)
+        own_column(2, False)
+        guest_scale()
+        guest_products(order[0])
+        pass_on(0, goals[3], 1)
+        hop(1, 1, (0, 1), False)
+        apart(feeder, (guest_pass, order[0]))
+        guest_products(order[1])
+        gating(0, y)
+        for third in order[:-1]:
+            convolve(0, y, third)
+        hop(2, 1, (0,), False)
+        apart(feeder, (guest_pass, order[1]))
+        gating(0, 1 - y)
+        hop(1, 1, (0, 1), True)
+        hop(2, 1, (1,), False)
+        apart(host, (guest_gate, order[0]))
+        for third in order[:-1]:
+            convolve(0, 1 - y, third)
+            normalise(0, third)
+        hop(1, 2)
+        own_rows(2)
+        apart(host, (guest_gate, order[1]))
+        guest_products(order[2])
+        apart(feeder, (guest_pass, order[2]))
+        side(1, 1)
+        side(1, 2)
+        apart(host, (guest_gate, order[2]))
+
+    apart(outer, (end_start,))
+    apart(middle, (middle_start,))
     end = outer.astype(jnp.int32)
     for level in range(layers):
         first, second = 2 * level, 2 * level + 1
         last = level == layers - 1
         targets = [target_of(turn_index) for turn_index in range(n_tp)]
         third_target = targets[2] * end + targets[3] * (1 - end)
-        contribute(level, targets[0], 0)
-        if level == 0:
-            hop(first, 1)
-        else:
-            apart(outer, (turn, first), (hop, first, 1, (1,)))
-        contribute(level, targets[1], 0)
-        apart(middle, (contribute, level, targets[2], 0))
-        contribute(level, targets[0], 1)
-        pass_on(level, targets[0], 0)
-        apart(middle, (side, first, 1))
-        if level == 0:
-            hop(first, 2)
-        else:
-            apart(outer, (hop, first, 2))
-        pass_on(level, targets[1], 0)
-        apart(middle, (pass_on, level, targets[2], 0))
-        contribute(level, third_target, 0)
-        pass_on(level, targets[0], 1)
-        contribute(level, targets[1], 1)
-        apart(
-            outer,
-            (hop, first, 3),
-            (own_rows, second),
-            (contribute, level, targets[3], 0),
-        )
-        pass_on(level, third_target, 0)
-        pass_on(level, targets[1], 1)
-        contribute(level, targets[2], 1)
-        apart(outer, (pass_on, level, targets[3], 0))
-        pass_on(level, targets[2], 1)
-        apart(outer, (side, first, nz - 1))
-        apart(middle, (side, first, nz - 2), (own_rows, second), (own_column, second))
-        contribute(level, targets[3], 1)
-        pass_on(level, targets[3], 1)
-        apart(outer, (turn, second), (hop, second, 1), (hop, second, 2, (0,)))
-        apart(middle, (hop, second, 1))
-        row_scales(level)
-        gating(level, y)
-        for third in order[:-1]:
-            convolve(level, y, third)
-        apart(outer, (hop, second, 2, (1,)))
-        gating(level, 1 - y)
-        apart(middle, (hop, second, 2))
-        for third in order[:-1]:
-            convolve(level, 1 - y, third)
-            normalise(level, third)
-            if third == order[0]:
-                apart(outer, (hop, second, 3, (0,)))
-                if not last:
-                    apart(outer, (own_rows, first + 2))
-        apart(middle, (side, second, 1), (side, second, 2))
-        if not last:
-            apart(middle, (own_rows, first + 2), (own_column, first + 2))
+        if level > 0:
+            contribute(level, targets[0], 0)
+            contribute(level, targets[1], 0)
+            apart(middle, (contribute, level, targets[2], 0))
+            contribute(level, targets[0], 1)
+            pass_on(level, targets[0], 0)
+            apart(outer, (hop, first, 2, (1,)))
+            pass_on(level, targets[1], 0)
+            apart(middle, (pass_on, level, targets[2], 0))
+            contribute(level, third_target, 0)
+            pass_on(level, targets[0], 1)
+            contribute(level, targets[1], 1)
+            apart(
+                outer,
+                (hop, first, 3),
+                (own_rows, second),
+                (hop, second, 1),
+                (contribute, level, targets[3], 0),
+            )
+            pass_on(level, third_target, 0)
+            pass_on(level, targets[1], 1)
+            contribute(level, targets[2], 1)
+            apart(outer, (pass_on, level, targets[3], 0))
+            pass_on(level, targets[2], 1)
+            apart(outer, (side, first, nz - 1))
+            apart(middle, (side, first, nz - 2), (own_rows, second), (own_column, second, False))
+            contribute(level, targets[3], 1)
+            pass_on(level, targets[3], 1)
+            apart(outer, (turn, second))
+            apart(middle, (hop, second, 1))
+            row_scales(level)
+            gating(level, y)
+            for third in order[:-1]:
+                convolve(level, y, third)
+            apart(outer, (hop, second, 2, (0,)))
+            gating(level, 1 - y)
+            apart(middle, (hop, second, 2))
+            for third in order[:-1]:
+                convolve(level, 1 - y, third)
+                normalise(level, third)
+                if third == order[0]:
+                    apart(outer, (hop, second, 2, (1,)), (hop, second, 3, (0,)))
+            apart(middle, (side, second, 1), (side, second, 2))
         for block in (y, 1 - y):
             first_rows(level, block)
             convolve(level, block, order[-1])
         normalise(level, order[-1])
         relay(level, order[0])
-        apart(outer, (hop, second, 3, (1,)), (side, second, nz - 1))
+        if level > 0:
+            apart(outer, (hop, second, 3, (1,)), (side, second, nz - 1))
+        else:
+            apart(outer, (guest_left,), (side, second, nz - 1))
+        if not last:
+            apart(middle, (hop, first + 2, 1, (0,), True))
         for source in range(nz):
             crossed(second, source)
+        if not last:
+            apart(middle, (hop, first + 2, 1, (1,), True))
         for index in range(1, tiles):
             relay(level, order[index])
             projecting(level, order[index - 1])
-        if not last:
-            apart(middle, (hop, first + 2, 1))
-            apart(outer, (hop, first + 2, 1, (0,)))
         projecting(level, order[-1])
         if not last:
             for copy in square_copies(level + 1):
                 copy.start()
-            apart(middle, (hop, first + 2, 2))
+            apart(middle, (side, first + 2, 1), (hop, first + 2, 2))
         settle(level)
+    guest_settle()
     for phase in range(len(phases)):
         sent(phase)
+    for third in order:
+        result_copy(third).wait()
 
 
 def fused(n_sp, n_tp, *arrays):
@@ -672,18 +931,20 @@
     piece = value_proj.shape[2]
     blocks = n_sp // n_tp
     channels = blocks * piece
-    kinds = 3
+    kinds = 4
+    tiles = rows // ROW_TILE
     vmem = pl.BlockSpec(memory_space=pltpu.VMEM)
-    hbm = pl.BlockSpec(memory_space=pl.ANY)
+    hbm = pl.BlockSpec(memory_space=pltpu.HBM)
     low, wide = jnp.bfloat16, jnp.float32
-    slots = 4 * blocks + 3 * (rows // ROW_TILE)
+    slots = (3 + layers) * blocks + 3 * (rows // ROW_TILE)
     arrays = arrays[:4] + (arrays[4].transpose(1, 0, 2),) + arrays[5:]
     return pl.pallas_call(
         lambda *refs: fused_kernel(n_sp, n_tp, *refs),
         out_shape=jax.ShapeDtypeStruct((rows, feats), low),
-        in_specs=[vmem, vmem, hbm, hbm, vmem, vmem, vmem, vmem, hbm],
-        out_specs=vmem,
+        in_specs=[hbm, vmem, hbm, hbm, vmem, vmem, vmem, vmem, hbm],
+        out_specs=hbm,
         scratch_shapes=[
+            pltpu.VMEM((rows, feats), low),
             pltpu.VMEM((layers, n_sp, feats, 2 * piece), low),
             pltpu.VMEM((layers, n_sp * piece, feats), low),
             pltpu.VMEM((rows, feats), low),
@@ -699,13 +960,26 @@
             pltpu.VMEM((layers, n_tp, rows, channels), low),
             pltpu.VMEM((layers, n_tp, 8, rows), wide),
             pltpu.VMEM((rows, 8), wide),
+            pltpu.VMEM((rows, feats), low),
+            pltpu.VMEM((2, tiles, blocks, ROW_TILE, 2 * piece), low),
+            pltpu.VMEM((tiles, blocks, ROW_TILE, 2 * piece), low),
+            pltpu.VMEM((tiles, blocks, ROW_TILE, 2 * piece), low),
+            pltpu.VMEM((tiles, blocks, ROW_TILE, 2 * piece), low),
+            pltpu.VMEM((tiles, blocks, ROW_TILE, piece), low),
+            pltpu.VMEM((tiles, blocks, ROW_TILE, piece), low),
+            pltpu.VMEM((8, rows), wide),
+            pltpu.VMEM((8, rows), wide),
+            pltpu.VMEM((rows, 8), wide),
             pltpu.SemaphoreType.DMA((layers, kinds)),
-            pltpu.SemaphoreType.DMA((layers * 2, 2, 3, n_sp)),
+            pltpu.SemaphoreType.DMA((rows // ROW_TILE,)),
+            pltpu.SemaphoreType.DMA((layers * 2, 2 * n_sp + 4)),
             pltpu.SemaphoreType.DMA((layers * 2, 2, n_sp)),
-            pltpu.SemaphoreType.DMA((layers, slots)),
-            pltpu.SemaphoreType.DMA((layers, slots)),
-            pltpu.SemaphoreType.DMA((layers, 3)),
-            pltpu.SemaphoreType.DMA((layers, 3)),
+            pltpu.SemaphoreType.DMA((slots,)),
+            pltpu.SemaphoreType.DMA((slots,)),
+            pltpu.SemaphoreType.DMA((3,)),
+            pltpu.SemaphoreType.DMA((3,)),
+            pltpu.SemaphoreType.DMA((4 * tiles + 1,)),
+            pltpu.SemaphoreType.DMA((4 * tiles + 1,)),
         ],
         compiler_params=pltpu.CompilerParams(
             collective_id=0, has_side_effects=True, vmem_limit_bytes=VMEM_BYTES
@@ -716,7 +990,7 @@
 def solution(mesh):
     n_sp, n_tp = mesh.shape["sp"], mesh.shape["tp"]
     piece = C // n_sp
-    small = n_tp == 4 and GROUPS == n_tp and n_sp == 2 * n_tp and piece % 128 == 0
+    small = n_tp == 4 and GROUPS == n_tp and n_sp == 8 and piece % 128 == 0
 
     def local(*arrays):
         if small and arrays[0].shape[0] % ROW_TILE == 0:

time: 141 us -> 137 us (0.972)
  Pallas kernels: 139 us -> 134 us
    pallas_call x1, Pallas kernels: 139 us -> 134 us  [fused(): pl.pallas_call(lambda *refs: fused_kernel(n_sp, n_tp, *refs), out_shape=j...]
where the time goes in v3:
time: 137 us; the launch traced here: 136 us
  Pallas kernels  134 us (98%)
  local copies, waits for them, and re-layouts  2.67 us (2%)
    pallas_call x1, Pallas kernels, fused(): pl.pallas_call(lambda *refs: fused_kernel(n_sp, n_tp, *refs), out_shape=j...  134 us

profile of v3, /device:TPU:0, one launch (start us, length us, event | category | flops | bytes accessed | tf_op | source)
XLA Modules:
  0.0 136.4 jit_solution(15330569634293613022)
XLA Ops:
  0.0 133.8 %shard_map.91 = bf16[768,1024]{1,0:T(8,128)(2,1)} custom-call(bf16[768,1024]{1,0:T(8,128)(2,1)} %refs_0_.1, bf16[2,1024]{1,0:T(2,128)(2,1)} %refs_1_.1, bf16[2,1024,128]{2,1,0:T(8,128)(2,1)} %refs_2_.1, bf16[2,1024,128]{2,1,0:T(8,128)(2,1)} %refs_3_.1, bf16[31,2,256]{2,1,0:T(2,128)(2,1)} %bitcast.1, bf16[2,256]{1,0:T(2,128)(2,1)} %refs_5_.1, ...), custom_call_target="tpu_custom_call" | custom-call | tf_op jit(solution)/shard_map/pallas_call | solution.py:941
  133.8 2.7 %copy.11 = bf16[768,1024]{1,0:T(8,128)(2,1)} copy(bf16[768,1024]{1,0:T(8,128)(2,1)} %shard_map.91) | data formatting | bytes 3145728

commit v4 on v3

--- a/solution.py
+++ b/solution.py
@@ -426,21 +426,28 @@
         if level == 0:
             guest_sum[...] = total
 
-    def core_copy(level, target_chip, block):
+    def rows_of(third):
+        return pl.ds(pl.multiple_of(third * ROW_TILE, ROW_TILE), ROW_TILE)
+
+    def core_copy(level, target_chip, block, third):
         owner = target_chip * 2 + 1 - core
         return tp_copy(
             level,
-            target_chip * blocks + block,
-            part.at[owner, block],
-            from_core.at[level, target_chip, block],
+            (target_chip * blocks + block) * tiles + third,
+            part.at[owner, block, rows_of(third), :],
+            from_core.at[level, target_chip, block, rows_of(third), :],
             core_mate,
         )
 
-    base = 2 * blocks
-
-    def chip_copy(level, block):
+    base = 3 * blocks * tiles - blocks
+
+    def chip_copy(level, block, third):
         return tp_copy(
-            level, base + block, to_chip.at[block], from_chip.at[level, block], chip_mate
+            level,
+            (2 * blocks + block) * tiles + third,
+            to_chip.at[block, rows_of(third), :],
+            from_chip.at[level, block, rows_of(third), :],
+            chip_mate,
         )
 
     def halo_copy(level, block):
@@ -467,17 +474,18 @@
 
     def products(level, target, block):
         @pl.loop(0, tiles)
-        def _(tile):
-            span = pl.ds(pl.multiple_of(tile * ROW_TILE, ROW_TILE), ROW_TILE)
+        def _(step):
+            third = tiles - 1 - step
+            span = rows_of(third)
             part[target, block, span, :] = jnp.dot(
                 scaled[span, :],
                 w_in[level, target * blocks + block],
                 preferred_element_type=jnp.float32,
             ).astype(jnp.bfloat16)
 
-        @pl.when(target % 2 != core)
-        def _():
-            core_copy(level, target // 2, block).start()
+            @pl.when(target % 2 != core)
+            def _():
+                core_copy(level, target // 2, block, third).start()
 
     def contribute(level, target, turned):
         block = 1 - y if turned else y
@@ -490,39 +498,38 @@
 
         @pl.when(target == chip_mate)
         def _():
-            core_copy(level, 1 - chip, block).wait_recv()
-
             @pl.loop(0, tiles)
-            def _(tile):
-                span = pl.ds(pl.multiple_of(tile * ROW_TILE, ROW_TILE), ROW_TILE)
+            def _(step):
+                third = tiles - 1 - step
+                span = rows_of(third)
+                core_copy(level, 1 - chip, block, third).wait_recv()
                 to_chip[block, span, :] = (
                     part[chip_mate, block, span, :].astype(jnp.float32)
                     + from_core[level, 1 - chip, block, span, :].astype(jnp.float32)
                 ).astype(jnp.bfloat16)
-
-            chip_copy(level, block).start()
+                chip_copy(level, block, third).start()
+
+    def gate(level, block, third):
+        core_copy(level, chip, block, third).wait_recv()
+        chip_copy(level, block, third).wait_recv()
+        span = rows_of(third)
+        total = (
+            part[t, block, span, :].astype(jnp.float32)
+            + from_core[level, chip, block, span, :].astype(jnp.float32)
+            + from_chip[level, block, span, :].astype(jnp.float32)
+        ) * scales[span, 0:1]
+        gated = (total[:, :piece] * jax.nn.sigmoid(total[:, piece:])).astype(jnp.bfloat16)
+        extended[block, pl.ds(HALO + third * ROW_TILE, ROW_TILE), :] = gated.astype(jnp.float32)
+        if third == tiles - 1:
+            halo_send[block] = gated[ROW_TILE - HALO :]
+
+            @pl.when(s < n_sp - 1)
+            def _():
+                halo_copy(level, block).start()
 
     def gating(level, block):
-        core_copy(level, chip, block).wait_recv()
-        chip_copy(level, block).wait_recv()
-
-        @pl.loop(0, tiles)
-        def _(tile):
-            start = pl.multiple_of(tile * ROW_TILE, ROW_TILE)
-            span = pl.ds(start, ROW_TILE)
-            total = (
-                part[t, block, span, :].astype(jnp.float32)
-                + from_core[level, chip, block, span, :].astype(jnp.float32)
-                + from_chip[level, block, span, :].astype(jnp.float32)
-            ) * scales[span, 0:1]
-            gated = (total[:, :piece] * jax.nn.sigmoid(total[:, piece:])).astype(jnp.bfloat16)
-            extended[block, pl.ds(HALO + start, ROW_TILE), :] = gated.astype(jnp.float32)
-
-        halo_send[block] = extended[block, pl.ds(rows, HALO), :].astype(jnp.bfloat16)
-
-        @pl.when(s < n_sp - 1)
-        def _():
-            halo_copy(level, block).start()
+        for third in order:
+            gate(level, block, third)
 
     upper_half = z // (nz // 2)
     guest_chip = 1 - upper_half
@@ -555,8 +562,8 @@
         guest_copy(4, 0).start()
         for third in order[:-1]:
             guest_copy(0, third).start()
+        guest_copy(0, order[-1]).start()
         own_column(1)
-        guest_copy(0, order[-1]).start()
 
     def guest_left():
         guest_copy(4, 0).wait_send()
@@ -707,14 +714,16 @@
             @pl.when(jnp.logical_or(used, target_chip != guest_chip))
             def _(target_chip=target_chip):
                 for block in range(blocks):
-                    core_copy(level, target_chip, block).wait_send()
+                    for third in order:
+                        core_copy(level, target_chip, block, third).wait_send()
 
         passed = jnp.logical_or(middle, lender) if level == 0 else z >= 0
 
         @pl.when(passed)
         def _():
             for block in range(blocks):
-                chip_copy(level, block).wait_send()
+                for third in order:
+                    chip_copy(level, block, third).wait_send()
 
         for slot in range(3):
             for third in order:
@@ -763,6 +772,7 @@
         pass_on(0, goals[0], 1)
         pass_on(0, goals[1], 1)
         turn(1)
+        apart(jnp.logical_or(z > 0, y == 0), (own_column, 2))
         hop(1, 1)
         own_rows(2)
         apart(
@@ -782,13 +792,14 @@
             ),
         )
         apart(lender, (lend, order[0]))
-        own_column(2)
+        apart(jnp.logical_and(z == 0, y == 1), (own_column, 2))
         turn(2)
         apart(lender, (lend, order[1]), (late, order[0]))
-        hop(1, 3)
+        hop(1, 3, (0,))
+        hop(2, 2)
         own_column(3)
         apart(lender, (lend, order[2]), (late, order[1]))
-        hop(2, 2, (0,))
+        hop(1, 3, (1,))
 
     def middle_start():
         for phase in range(1, len(phases)):
@@ -799,12 +810,12 @@
         contribute(0, goals[2], 0)
         contribute(0, goals[0], 1)
         pass_on(0, goals[0], 0)
+        pass_on(0, goals[1], 0)
+        pass_on(0, goals[2], 0)
         side(0, 1)
         hop(0, 2)
         own_rows(1)
         own_column(1, False)
-        pass_on(0, goals[1], 0)
-        pass_on(0, goals[2], 0)
         contribute(0, goals[3], 0)
         pass_on(0, goals[0], 1)
         contribute(0, goals[1], 1)
@@ -817,81 +828,78 @@
         own_column(2, False)
         guest_scale()
         guest_products(order[0])
-        pass_on(0, goals[3], 1)
         hop(1, 1, (0, 1), False)
         apart(feeder, (guest_pass, order[0]))
+        pass_on(0, goals[3], 1)
         guest_products(order[1])
         gating(0, y)
         for third in order[:-1]:
             convolve(0, y, third)
         hop(2, 1, (0,), False)
         apart(feeder, (guest_pass, order[1]))
+        hop(2, 1, (1,), False)
+        own_column(3, False)
+        apart(host, (guest_gate, order[0]))
         gating(0, 1 - y)
-        hop(1, 1, (0, 1), True)
-        hop(2, 1, (1,), False)
-        apart(host, (guest_gate, order[0]))
+        guest_products(order[2])
+        apart(feeder, (guest_pass, order[2]))
+        hop(1, 1, (0,), True)
         for third in order[:-1]:
             convolve(0, 1 - y, third)
             normalise(0, third)
-        hop(1, 2)
+        apart(host, (guest_gate, order[1]))
+        hop(1, 1, (1,), True)
+        hop(1, 2, (0,))
         own_rows(2)
-        apart(host, (guest_gate, order[1]))
-        guest_products(order[2])
-        apart(feeder, (guest_pass, order[2]))
         side(1, 1)
+        hop(1, 2, (1,))
+        apart(host, (guest_gate, order[2]))
         side(1, 2)
-        apart(host, (guest_gate, order[2]))
+        hop(2, 1, (0,), True)
+        hop(3, 1, (0, 1), False)
 
     apart(outer, (end_start,))
     apart(middle, (middle_start,))
-    end = outer.astype(jnp.int32)
     for level in range(layers):
         first, second = 2 * level, 2 * level + 1
         last = level == layers - 1
         targets = [target_of(turn_index) for turn_index in range(n_tp)]
-        third_target = targets[2] * end + targets[3] * (1 - end)
         if level > 0:
+            apart(outer, (hop, first, 3, (0,)), (own_rows, second), (hop, second, 1))
             contribute(level, targets[0], 0)
             contribute(level, targets[1], 0)
-            apart(middle, (contribute, level, targets[2], 0))
+            apart(middle, (hop, second, 1, (0, 1), True))
             contribute(level, targets[0], 1)
             pass_on(level, targets[0], 0)
-            apart(outer, (hop, first, 2, (1,)))
+            contribute(level, targets[2], 0)
             pass_on(level, targets[1], 0)
-            apart(middle, (pass_on, level, targets[2], 0))
-            contribute(level, third_target, 0)
             pass_on(level, targets[0], 1)
             contribute(level, targets[1], 1)
-            apart(
-                outer,
-                (hop, first, 3),
-                (own_rows, second),
-                (hop, second, 1),
-                (contribute, level, targets[3], 0),
-            )
-            pass_on(level, third_target, 0)
+            pass_on(level, targets[2], 0)
+            apart(middle, (side, first, nz - 2))
+            contribute(level, targets[2], 1)
             pass_on(level, targets[1], 1)
-            contribute(level, targets[2], 1)
-            apart(outer, (pass_on, level, targets[3], 0))
             pass_on(level, targets[2], 1)
+            apart(outer, (turn, second), (hop, first, 3, (1,)))
+            contribute(level, targets[3], 0)
+            apart(outer, (hop, second, 2))
+            apart(middle, (own_rows, second))
+            pass_on(level, targets[3], 0)
             apart(outer, (side, first, nz - 1))
-            apart(middle, (side, first, nz - 2), (own_rows, second), (own_column, second, False))
             contribute(level, targets[3], 1)
             pass_on(level, targets[3], 1)
-            apart(outer, (turn, second))
-            apart(middle, (hop, second, 1))
+            apart(middle, (hop, second, 2))
             row_scales(level)
             gating(level, y)
             for third in order[:-1]:
                 convolve(level, y, third)
-            apart(outer, (hop, second, 2, (0,)))
-            gating(level, 1 - y)
-            apart(middle, (hop, second, 2))
-            for third in order[:-1]:
-                convolve(level, 1 - y, third)
-                normalise(level, third)
-                if third == order[0]:
-                    apart(outer, (hop, second, 2, (1,)), (hop, second, 3, (0,)))
+            gate(level, 1 - y, order[0])
+            for index in range(1, tiles):
+                gate(level, 1 - y, order[index])
+                convolve(level, 1 - y, order[index - 1])
+                normalise(level, order[index - 1])
+                if index == 1:
+                    apart(outer, (hop, second, 3, (0,)))
             apart(middle, (side, second, 1), (side, second, 2))
         for block in (y, 1 - y):
             first_rows(level, block)
@@ -902,8 +910,6 @@
             apart(outer, (hop, second, 3, (1,)), (side, second, nz - 1))
         else:
             apart(outer, (guest_left,), (side, second, nz - 1))
-        if not last:
-            apart(middle, (hop, first + 2, 1, (0,), True))
         for source in range(nz):
             crossed(second, source)
         if not last:
@@ -911,11 +917,15 @@
         for index in range(1, tiles):
             relay(level, order[index])
             projecting(level, order[index - 1])
+            if not last and index == 1:
+                apart(middle, (hop, first + 2, 2, (0,)))
+            if not last and index == 2:
+                apart(middle, (side, first + 2, 1))
         projecting(level, order[-1])
         if not last:
             for copy in square_copies(level + 1):
                 copy.start()
-            apart(middle, (side, first + 2, 1), (hop, first + 2, 2))
+            apart(middle, (hop, first + 2, 2, (1,)))
         settle(level)
     guest_settle()
     for phase in range(len(phases)):
@@ -936,7 +946,7 @@
     vmem = pl.BlockSpec(memory_space=pltpu.VMEM)
     hbm = pl.BlockSpec(memory_space=pltpu.HBM)
     low, wide = jnp.bfloat16, jnp.float32
-    slots = (3 + layers) * blocks + 3 * (rows // ROW_TILE)
+    slots = layers * blocks + 3 * (blocks + 1) * (rows // ROW_TILE)
     arrays = arrays[:4] + (arrays[4].transpose(1, 0, 2),) + arrays[5:]
     return pl.pallas_call(
         lambda *refs: fused_kernel(n_sp, n_tp, *refs),

time: 137 us -> 130 us (0.949)
  Pallas kernels: 134 us -> 127 us
    pallas_call x1, Pallas kernels: 134 us -> 127 us  [fused(): pl.pallas_call(lambda *refs: fused_kernel(n_sp, n_tp, *refs), out_shape=j...]
where the time goes in v4:
time: 130 us
  Pallas kernels  127 us (98%)
  local copies, waits for them, and re-layouts  2.67 us (2%)
    pallas_call x1, Pallas kernels, fused(): pl.pallas_call(lambda *refs: fused_kernel(n_sp, n_tp, *refs), out_shape=j...  127 us
    unnamed x1, local copies, waits for them, and re-layouts  2.67 us

profile of v4, /device:TPU:0, one launch (start us, length us, event | category | flops | bytes accessed | tf_op | source)
XLA Modules:
  0.0 129.9 jit_solution(1252415092780247639)
XLA Ops:
  0.0 127.2 %shard_map.91 = bf16[768,1024]{1,0:T(8,128)(2,1)} custom-call(bf16[768,1024]{1,0:T(8,128)(2,1)} %refs_0_.1, bf16[2,1024]{1,0:T(2,128)(2,1)} %refs_1_.1, bf16[2,1024,128]{2,1,0:T(8,128)(2,1)} %refs_2_.1, bf16[2,1024,128]{2,1,0:T(8,128)(2,1)} %refs_3_.1, bf16[31,2,256]{2,1,0:T(2,128)(2,1)} %bitcast.1, bf16[2,256]{1,0:T(2,128)(2,1)} %refs_5_.1, ...), custom_call_target="tpu_custom_call" | custom-call | tf_op jit(solution)/shard_map/pallas_call | solution.py:951
  127.2 2.7 %copy.11 = bf16[768,1024]{1,0:T(8,128)(2,1)} copy(bf16[768,1024]{1,0:T(8,128)(2,1)} %shard_map.91) | data formatting | bytes 3145728

commit v5 on v4

--- a/solution.py
+++ b/solution.py
@@ -796,8 +796,9 @@
         turn(2)
         apart(lender, (lend, order[1]), (late, order[0]))
         hop(1, 3, (0,))
-        hop(2, 2)
+        hop(2, 2, (0,))
         own_column(3)
+        own_rows(3)
         apart(lender, (lend, order[2]), (late, order[1]))
         hop(1, 3, (1,))
 
@@ -837,7 +838,6 @@
             convolve(0, y, third)
         hop(2, 1, (0,), False)
         apart(feeder, (guest_pass, order[1]))
-        hop(2, 1, (1,), False)
         own_column(3, False)
         apart(host, (guest_gate, order[0]))
         gating(0, 1 - y)
@@ -851,12 +851,12 @@
         hop(1, 1, (1,), True)
         hop(1, 2, (0,))
         own_rows(2)
+        apart(host, (guest_gate, order[2]))
         side(1, 1)
         hop(1, 2, (1,))
-        apart(host, (guest_gate, order[2]))
         side(1, 2)
+        hop(2, 1, (1,), False)
         hop(2, 1, (0,), True)
-        hop(3, 1, (0, 1), False)
 
     apart(outer, (end_start,))
     apart(middle, (middle_start,))
@@ -865,34 +865,35 @@
         last = level == layers - 1
         targets = [target_of(turn_index) for turn_index in range(n_tp)]
         if level > 0:
-            apart(outer, (hop, first, 3, (0,)), (own_rows, second), (hop, second, 1))
+            contribute(level, targets[2], 0)
             contribute(level, targets[0], 0)
+            pass_on(level, targets[2], 0)
             contribute(level, targets[1], 0)
+            pass_on(level, targets[0], 0)
+            apart(outer, (hop, first, 3, (0,)), (hop, second, 1), (turn, second))
             apart(middle, (hop, second, 1, (0, 1), True))
             contribute(level, targets[0], 1)
-            pass_on(level, targets[0], 0)
-            contribute(level, targets[2], 0)
             pass_on(level, targets[1], 0)
+            apart(middle, (side, first, nz - 2), (hop, second, 1, (0, 1), False))
+            contribute(level, targets[2], 1)
             pass_on(level, targets[0], 1)
             contribute(level, targets[1], 1)
-            pass_on(level, targets[2], 0)
-            apart(middle, (side, first, nz - 2))
-            contribute(level, targets[2], 1)
+            pass_on(level, targets[2], 1)
+            apart(middle, (side, second, 1))
             pass_on(level, targets[1], 1)
-            pass_on(level, targets[2], 1)
-            apart(outer, (turn, second), (hop, first, 3, (1,)))
+            apart(outer, (hop, first, 3, (1,)))
             contribute(level, targets[3], 0)
-            apart(outer, (hop, second, 2))
-            apart(middle, (own_rows, second))
+            apart(middle, (own_rows, second), (hop, second, 2))
             pass_on(level, targets[3], 0)
             apart(outer, (side, first, nz - 1))
             contribute(level, targets[3], 1)
             pass_on(level, targets[3], 1)
-            apart(middle, (hop, second, 2))
+            apart(middle, (side, second, 2))
             row_scales(level)
             gating(level, y)
             for third in order[:-1]:
                 convolve(level, y, third)
+            apart(outer, (hop, second, 2))
             gate(level, 1 - y, order[0])
             for index in range(1, tiles):
                 gate(level, 1 - y, order[index])
@@ -900,7 +901,6 @@
                 normalise(level, order[index - 1])
                 if index == 1:
                     apart(outer, (hop, second, 3, (0,)))
-            apart(middle, (side, second, 1), (side, second, 2))
         for block in (y, 1 - y):
             first_rows(level, block)
             convolve(level, block, order[-1])
@@ -919,6 +919,7 @@
             projecting(level, order[index - 1])
             if not last and index == 1:
                 apart(middle, (hop, first + 2, 2, (0,)))
+                apart(outer, (hop, first + 2, 2, (1,)))
             if not last and index == 2:
                 apart(middle, (side, first + 2, 1))
         projecting(level, order[-1])

time: 130 us -> 129 us (level)
  Pallas kernels: 127 us -> 125 us
    pallas_call x1, Pallas kernels: 127 us -> 125 us  [fused(): pl.pallas_call(lambda *refs: fused_kernel(n_sp, n_tp, *refs), out_shape=j...]
where the time goes in v5:
time: 129 us; the launch traced here: 128 us
  Pallas kernels  125 us (97%)
  local copies, waits for them, and re-layouts  2.67 us (2%)
    pallas_call x1, Pallas kernels, fused(): pl.pallas_call(lambda *refs: fused_kernel(n_sp, n_tp, *refs), out_shape=j...  125 us
    unnamed x1, local copies, waits for them, and re-layouts  2.67 us

profile of v5, /device:TPU:0, one launch (start us, length us, event | category | flops | bytes accessed | tf_op | source)
XLA Modules:
  0.0 127.7 jit_solution(12621829107425276747)
XLA Ops:
  0.0 125.0 %shard_map.91 = bf16[768,1024]{1,0:T(8,128)(2,1)} custom-call(bf16[768,1024]{1,0:T(8,128)(2,1)} %refs_0_.1, bf16[2,1024]{1,0:T(2,128)(2,1)} %refs_1_.1, bf16[2,1024,128]{2,1,0:T(8,128)(2,1)} %refs_2_.1, bf16[2,1024,128]{2,1,0:T(8,128)(2,1)} %refs_3_.1, bf16[31,2,256]{2,1,0:T(2,128)(2,1)} %bitcast.1, bf16[2,256]{1,0:T(2,128)(2,1)} %refs_5_.1, ...), custom_call_target="tpu_custom_call" | custom-call | tf_op jit(solution)/shard_map/pallas_call | solution.py:952
  125.0 2.7 %copy.11 = bf16[768,1024]{1,0:T(8,128)(2,1)} copy(bf16[768,1024]{1,0:T(8,128)(2,1)} %shard_map.91) | data formatting | bytes 3145728
